TPU v7x, 128 devices: a whole 4x4x4 slice. The times are simulated.
128 devices in a mesh: sp: 16 (over z, x), tp: 8 (over y, core).
Axes of the slice: x: 4, y: 4, z: 4, core: 2. Of those that a mesh axis runs over, the one named last changes fastest.
Arguments:
- resid: bfloat16 [12288, 3072], P('sp', 'tp'), may hold values from -12 to 12
- query: bfloat16 [12288, 1536], P('sp', 'tp'), may hold values from -6 to 6
- keys: bfloat16 [12288, 1536], P('sp', 'tp'), may hold values from -6 to 6
- values: bfloat16 [12288, 1536], P('sp', 'tp'), may hold values from -6 to 6
- out_gate: bfloat16 [12288, 1536], P('sp', 'tp'), may hold values from -6 to 6
- in_gate: float32 [16, 12288], P('tp', 'sp'), may hold values from -6 to 110
- forget: float32 [16, 12288], P('tp', 'sp'), may hold values from -1 to 16
- doc_ids: int32 [12288], P('sp'), may hold values from 0 to 7, never falling along the last dimension, each value on 1 to 3072 neighbouring positions
- head_gain: float32 [1536], P('tp'), may hold values from 0.1 to 1.9
- w_out: bfloat16 [1536, 3072], P('tp'), may hold values from -0.15625 to 0.15625
- ffn_gain: float32 [3072], replicated, may hold values from 0.1 to 1.9
- w_gate: bfloat16 [3072, 8448], P('sp', 'tp'), may hold values from -0.109375 to 0.109375
- w_value: bfloat16 [3072, 8448], P('sp', 'tp'), may hold values from -0.109375 to 0.109375
- conv_taps: float32 [3, 8448], P(None, 'tp'), may hold values from -3.5 to 3.5
- w_down: bfloat16 [8448, 3072], P('tp', 'sp'), may hold values from -0.0625 to 0.0625
Outputs:
- layer_out: bfloat16 [12288, 3072], P('sp', 'tp')
Inputs may be any that keep to these rules, and one draw needn't show every extreme that they name: `doc_ids`: document numbers never fall along the positions; each document is 1 to 3072 positions long.
All inputs are finite; a program needn't handle non-finite values.
Results may differ from a plain program's by a relative error of at most 0.02.
Values may be sent and summed in bfloat16 or wider, within the bound.
No kernel may reach another device: no remote copies, remote signals or barrier semaphores. Data moves between devices by JAX's collectives and lax.ppermute only.
A program may use at most 128 MiB of HBM per device.

v0:
```python
import jax
import jax.numpy as jnp
from jax import lax
from jax.experimental import pallas as pl
from jax.experimental.pallas import tpu as pltpu
from jax.sharding import Mesh
from jax.sharding import PartitionSpec as P


DH = 96
DOC_MAX = 3072
SP = ("z", "x")
TP = ("y", "c")
ABSENT = -1e30
HALO = 16
EPS = 1e-06
HEAD_FLOOR = 1.0
F32 = jnp.float32
BF16 = jnp.bfloat16


def in_first_head(shape):
    return lax.broadcasted_iota(jnp.int32, shape, len(shape) - 1) < DH


def pack_kernel(gate_ref, value_ref, down_ref, out_ref):
    rows, hidden = gate_ref.shape
    main = hidden // 128 * 128
    tails = []
    for k, ref in enumerate((gate_ref, value_ref, down_ref)):
        out_ref[:, k * main : (k + 1) * main] = ref[:, :main]
        tails.append(ref[:, main:])
    tails.append(jnp.zeros((rows, 128 - 3 * (hidden - main)), BF16))
    out_ref[:, 3 * main :] = jnp.concatenate(tails, axis=1)


def state_kernel(k_ref, v_ref, in_ref, forget_ref, doc_ref, pay_ref, row_ref, col_ref, scr):
    tokens, width = k_ref.shape
    lane = lax.broadcasted_iota(jnp.int32, (8, tokens), 1)
    doc = jnp.broadcast_to(doc_ref[...].astype(F32), (8, tokens))
    scr[...] = jnp.zeros_like(scr)
    scr[0:2, :] = forget_ref[...]
    raw = scr[...]
    total = jnp.minimum(raw, 0.0) - jnp.log1p(jnp.exp(-jnp.abs(raw)))
    step = 1
    while step < tokens:
        total = total + jnp.where(lane >= step, pltpu.roll(total, step, 1), 0.0)
        step *= 2
    scr[0:2, :] = in_ref[...]
    rest = scr[...] - total
    peak = rest
    step = 1
    while step < tokens:
        near = (lane >= step) & (pltpu.roll(doc, step, 1) == doc)
        peak = jnp.maximum(peak, jnp.where(near, pltpu.roll(peak, step, 1), ABSENT))
        step *= 2
    end_doc = doc[:, tokens - 1 : tokens]
    end_peak = peak[:, tokens - 1 : tokens]
    end_total = total[:, tokens - 1 : tokens]
    weight = jnp.where(doc == end_doc, jnp.exp(jnp.minimum(rest - end_peak, 0.0)), 0.0)
    row_ref[...] = jnp.zeros_like(row_ref)
    row_ref[0:2, :] = total[0:2, :]
    row_ref[2:4, :] = peak[0:2, :]
    row_ref[4:6, :] = weight[0:2, :]
    row_ref[6:7, :] = doc[0:1, :]
    scr[...] = row_ref[...]
    cols = scr[...].T
    col_ref[...] = cols
    row_ref[4:6, :] = rest[0:2, :]
    first = in_first_head((tokens, width))
    spread = jnp.where(first, cols[:, 4:5], cols[:, 5:6])
    weighted = (k_ref[...].astype(F32) * (spread * DH**-0.5)).astype(BF16)
    state = lax.dot_general(
        weighted, v_ref[...], (((0,), (0,)), ((), ())), preferred_element_type=F32
    )
    small = in_first_head((DH, width))
    pay_ref[0:DH, :] = jnp.where(small, state[0:DH, :], state[DH:, :]).astype(BF16)

    line = in_first_head((1, width))

    def spread_heads(x):
        return jnp.where(line, x[0:1, :], x[1:2, :])

    def split(x):
        high = x.astype(BF16).astype(F32)
        mid = (x - high).astype(BF16).astype(F32)
        return high, mid, x - high - mid

    lines = [
        *split(spread_heads(end_total + end_peak)),
        *split(spread_heads(end_total)),
        jnp.broadcast_to(end_doc[0:1, :] + 1.0, (1, width)),
        jnp.broadcast_to(doc[0:1, tokens - 2 : tokens - 1] + 1.0, (1, width)),
    ]
    place = lax.broadcasted_iota(jnp.int32, (16, width), 0)
    table = jnp.zeros((16, width), F32)
    for k, value in enumerate(lines):
        table = jnp.where(place == k, value, table)
    pay_ref[DH:, :] = table.astype(BF16)


def local_kernel(q_ref, k_ref, v_ref, row_ref, col_ref, out_ref):
    tokens, width = q_ref.shape
    block = 256
    for start in range(0, tokens, block):
        stop = start + block
        keys = k_ref[0:stop, :]
        vals = v_ref[0:stop, :]
        q = q_ref[start:stop, :]
        first = in_first_head((block, width))
        at = lax.broadcasted_iota(jnp.int32, (block, stop), 0) + start
        source = lax.broadcasted_iota(jnp.int32, (block, stop), 1)
        seen = (at >= source) & (row_ref[6:7, 0:stop] == col_ref[start:stop, 6:7])
        found = []
        for h in range(2):
            mine = jnp.where(first if h == 0 else jnp.logical_not(first), q, jnp.zeros_like(q))
            scores = lax.dot_general(
                mine, keys, (((1,), (1,)), ((), ())), preferred_element_type=F32
            )
            gap = row_ref[4 + h : 5 + h, 0:stop] - col_ref[start:stop, 2 + h : 3 + h]
            part = (scores * jnp.exp(jnp.where(seen, gap, ABSENT))).astype(BF16)
            found.append(jnp.dot(part, vals, preferred_element_type=F32))
        out_ref[start:stop, :] = jnp.where(first, found[0], found[1])


def mix_kernel(
    order_ref, q_ref, gate_ref, local_ref, row_ref, col_ref, gain_ref, w_ref, *refs
):
    w_own_ref, *pays = refs[:-5]
    swap_ref, own_out_ref, near_ref, far_ref, mix_ref = refs[-5:]
    tokens, width = q_ref.shape

    @pl.when(pl.program_id(0) == 0)
    def _():
        own = row_ref[6:7, 0:1] + 1.0
        behind = jnp.zeros((1, width), F32)
        peaks, goods = [], []
        for ref in pays:
            table = ref[DH:, :].astype(F32)
            good = table[6:7, :] == own
            peaks.append(
                jnp.where(good, table[0:1, :] + table[1:2, :] + table[2:3, :] + behind, ABSENT)
            )
            goods.append(good)
            behind = behind + (table[3:4, :] + table[4:5, :] + table[5:6, :])
        best = peaks[0]
        for value in peaks[1:]:
            best = jnp.maximum(best, value)
        state = jnp.zeros((DH, width), F32)
        for ref, value, good in zip(pays, peaks, goods):
            state = state + jnp.where(good, jnp.exp(value - best), 0.0) * ref[0:DH, :].astype(F32)
        small = in_first_head((DH, width))
        whole = jnp.concatenate(
            [jnp.where(small, state, 0.0), jnp.where(small, 0.0, state)], axis=0
        ).astype(BF16)
        carried = jnp.dot(q_ref[...], whole, preferred_element_type=F32)
        first = in_first_head((tokens, width))
        total = jnp.where(first, col_ref[:, 0:1], col_ref[:, 1:2])
        peak = total + jnp.where(first, col_ref[:, 2:3], col_ref[:, 3:4])
        inter = jnp.where(col_ref[:, 6:7] + 1.0 == own, total + best, ABSENT)
        top = jnp.maximum(peak, inter)
        memory = (
            jnp.exp(peak - top) * (local_ref[...] * DH**-0.5) + jnp.exp(inter - top) * carried
        )
        square = memory * memory
        mean_0 = jnp.sum(jnp.where(first, square, 0.0), axis=1, keepdims=True) / DH
        mean_1 = jnp.sum(jnp.where(first, 0.0, square), axis=1, keepdims=True) / DH
        norm = jnp.where(first, lax.rsqrt(mean_0 + HEAD_FLOOR), lax.rsqrt(mean_1 + HEAD_FLOOR))
        gate = gate_ref[...].astype(F32)
        mix_ref[...] = (memory * norm * gain_ref[...] * (1.0 / (1.0 + jnp.exp(-gate)))).astype(BF16)

        ids = pays[0][DH:, :].astype(F32)
        last, second = ids[6:7, 0:1], ids[7:8, 0:1]
        doc = jnp.broadcast_to(col_ref[:, 6:7], (tokens, 128)) + 1.0
        row = lax.broadcasted_iota(jnp.int32, (tokens, 128), 0)
        one = jnp.where(row == 0, last, pltpu.roll(doc, 1, 0))
        two = jnp.where(row == 0, second, jnp.where(row == 1, last, pltpu.roll(doc, 2, 0)))
        near_ref[...] = (one == doc).astype(F32)
        far_ref[...] = (two == doc).astype(F32)

    mix = mix_ref[...]
    swap_ref[0] = jnp.dot(mix, w_ref[...], preferred_element_type=F32).astype(BF16)
    own_out_ref[0] = jnp.dot(mix, w_own_ref[...], preferred_element_type=F32).astype(BF16)


def norm_kernel(order_ref, *refs):
    pieces, (gain_ref, out_ref, send_ref) = refs[:-3], refs[-3:]
    tokens, cols = pieces[0].shape
    model = out_ref.shape[1]
    i = pl.program_id(0)
    square = jnp.zeros((tokens, cols), F32)
    for ref in pieces:
        r = ref[...].astype(F32)
        square = square + r * r
    mean = jnp.sum(square, axis=1, keepdims=True) / model
    scale = lax.rsqrt(mean + EPS)
    rows = pl.ds(pl.multiple_of(HALO + i * tokens, 16), tokens)
    for p, ref in enumerate(pieces):
        cut = pl.ds(pl.multiple_of(order_ref[p] * cols, 128), cols)
        done = (ref[...].astype(F32) * scale * gain_ref[0:1, cut]).astype(BF16)
        out_ref[rows, cut] = done
        send_ref[:, cut] = done[tokens - HALO :, :]


def mixer_kernel(
    order_ref,
    x_ref,
    near_ref,
    far_ref,
    taps_ref,
    wg_ref,
    wv_ref,
    wt_ref,
    w_ref,
    h_ref,
    swap_ref,
    own_ref,
    gate_scr,
    value_scr,
    tail_scr,
    down_scr,
    sems,
):
    tokens = near_ref.shape[0]
    tiles, _, tile = taps_ref.shape
    tiles -= 1
    main = tiles * tile
    pairs, cols = down_scr.shape[0], down_scr.shape[1] // 2
    j = pl.program_id(0)

    def copies(n):
        rows = pl.ds(pl.multiple_of(order_ref[n] * cols, 128), cols)
        spot = down_scr.at[n // 2, pl.ds(n % 2 * cols, cols)]
        return (
            pltpu.make_async_copy(
                w_ref.at[rows, pl.ds(2 * main, main)],
                spot.at[:, pl.ds(0, main)],
                sems.at[2 * n],
            ),
            pltpu.make_async_copy(
                w_ref.at[rows, pl.ds(3 * main, 128)],
                spot.at[:, pl.ds(main, 128)],
                sems.at[2 * n + 1],
            ),
        )

    def hidden(gate, value, taps, rows):
        near, far = near_ref[rows, :], far_ref[rows, :]
        one = pltpu.roll(gate, 1, 0)[HALO:, :]
        two = pltpu.roll(gate, 2, 0)[HALO:, :]
        conv = (
            taps[2:3, :] * gate[HALO:, :]
            + taps[1:2, :] * (near * one)
            + taps[0:1, :] * (far * two)
        )
        scaled = 0.5 * conv
        return (scaled + scaled * jnp.tanh(scaled)) * value

    block = 96

    def finish(slot, at):
        for start in range(0, tokens, block):
            for half in range(0, tile, 128):
                lanes = slice(half, half + 128)
                done = hidden(
                    gate_scr[slot, start : start + block + HALO, lanes],
                    value_scr[slot, start + HALO : start + HALO + block, lanes],
                    taps_ref[at, :, lanes],
                    slice(start, start + block),
                )
                spot = at * tile + half
                if not isinstance(at, int):
                    spot = pl.multiple_of(spot, 128)
                h_ref[start : start + block, pl.ds(spot, 128)] = done.astype(BF16)

    def finish_tail():
        for start in range(0, tokens, block):
            part = tail_scr[start : start + block + HALO, :]
            lane = lax.broadcasted_iota(jnp.int32, (block, 128), 1)
            mine = (lane >= 64) & (lane < 96)
            done = hidden(
                pltpu.roll(part, 64, 1),
                pltpu.roll(part, 32, 1)[HALO:, :],
                taps_ref[tiles, :, 0:128],
                slice(start, start + block),
            )
            h_ref[start : start + block, main:] = jnp.where(mine, done, 0.0).astype(BF16)

    def project(slot):
        gate_scr[slot] = jnp.dot(x_ref[...], wg_ref[...], preferred_element_type=F32)
        value_scr[slot] = jnp.dot(x_ref[...], wv_ref[...], preferred_element_type=F32)

    def product(n, cuts):
        total = None
        for cut in cuts:
            term = lax.dot_general(
                h_ref[:, cut],
                down_scr[n, :, cut],
                (((1,), (1,)), ((), ())),
                preferred_element_type=F32,
            )
            total = term if total is None else total + term
        return total.astype(BF16)

    @pl.when(j == 0)
    def _():
        for n in range(2 * pairs):
            for copy in copies(n):
                copy.start()
        tail_scr[...] = jnp.dot(x_ref[...], wt_ref[...], preferred_element_type=F32)
        project(0)

    @pl.when(j == 1)
    def _():
        project(1)
        finish_tail()
        finish(0, 0)

    @pl.when((j > 1) & (j < tiles))
    def _():
        project(j % 2)
        finish((j - 1) % 2, j - 1)

    @pl.when(j == tiles)
    def _():
        finish((tiles - 1) % 2, tiles - 1)
        for n in range(2):
            for copy in copies(n):
                copy.wait()
        known = main - tile
        both = product(0, (slice(0, known), slice(main, main + 128), slice(known, main)))
        swap_ref[0], own_ref[0] = both[:, :cols], both[:, cols:]

    @pl.when(j > tiles)
    def _():
        for n in range(2, 4):
            for copy in copies(n):
                copy.wait()
        both = product(1, (slice(None),))
        swap_ref[1], swap_ref[2] = both[:, :cols], both[:, cols:]


def two_parts(h_ref, wa_ref, wb_ref, ta_ref, tb_ref):
    main = wa_ref.shape[1]
    contract = (((1,), (1,)), ((), ()))
    main_w = jnp.concatenate([wa_ref[...], wb_ref[...]], axis=0)
    tail_w = jnp.concatenate([ta_ref[...], tb_ref[...]], axis=0)
    both = lax.dot_general(
        h_ref[:, :main], main_w, contract, preferred_element_type=F32
    ) + lax.dot_general(h_ref[:, main:], tail_w, contract, preferred_element_type=F32)
    cols = wa_ref.shape[0]
    return both[:, :cols], both[:, cols:]


def side_kernel(order_ref, h_ref, wa_ref, wb_ref, ta_ref, tb_ref, a_ref, b_ref, up_ref, down_ref):
    up, down = two_parts(h_ref, wa_ref, wb_ref, ta_ref, tb_ref)
    up_ref[...] = (up + a_ref[0].astype(F32)).astype(BF16)
    down_ref[...] = (down + b_ref[0].astype(F32)).astype(BF16)


def down_kernel(order_ref, h_ref, wa_ref, wb_ref, ta_ref, tb_ref, swap_ref, own_ref):
    swap, own = two_parts(h_ref, wa_ref, wb_ref, ta_ref, tb_ref)
    swap_ref[...] = swap.astype(BF16)
    own_ref[...] = own.astype(BF16)


def added(*terms):
    total = terms[0].astype(F32)
    for term in terms[1:]:
        total = total + term.astype(F32)
    return total


def shifted(value, by):
    ring = lax.axis_size("y")
    return lax.ppermute(value, "y", [(i, (i + by) % ring) for i in range(ring)])


def swapped(value):
    return lax.ppermute(value, "c", [(0, 1), (1, 0)])


def summed_over_tp(swap, own, sides, last):
    other = swapped(swap)
    far = added(own, other[0]).astype(BF16)
    half = far.shape[0] // 2
    far_up, far_down = shifted(far[:half], 1), shifted(far[half:], -1)
    up, down = sides(other)
    below, above = shifted(up[half:], 1), shifted(down[:half], -1)
    up = added(up[:half], far_up).astype(BF16)
    down = added(down[half:], far_down).astype(BF16)
    up, down = shifted(up, 1), shifted(down, -1)
    swap, own = last()
    near = added(own, swapped(swap))
    return added(near[:half], up, above), added(near[half:], below, down)


def gathered_over_tp(own):
    half = own.shape[0] // 2
    below, above = shifted(own, 1), shifted(own, -1)
    far = jnp.concatenate([shifted(below[:half], 1), shifted(above[half:], -1)], axis=0)
    mine = [own, below, above, far]
    return mine + [swapped(part) for part in mine]


def shape(dims, dtype):
    return jax.ShapeDtypeStruct(dims, dtype)


def whole(dims):
    return pl.BlockSpec(dims, lambda *_: (0,) * len(dims))


def layer(
    resid,
    query,
    keys,
    values,
    out_gate,
    in_gate,
    forget,
    doc_ids,
    head_gain,
    w_out,
    ffn_gain,
    w_gate,
    w_value,
    conv_taps,
    w_down,
):
    tokens, width = query.shape
    cols = resid.shape[1]
    model = w_out.shape[1]
    hidden = w_gate.shape[1]
    main = hidden // 128 * 128
    spare = hidden - main
    packed = pl.pallas_call(
        pack_kernel,
        out_shape=shape((w_gate.shape[0], 3 * main + 128), BF16),
        name="pack",
    )(w_gate, w_value, w_down.T)
    weights = lax.all_gather(packed, SP, axis=0, tiled=True)
    tile = 256
    tiles = main // tile
    spot = 2 * spare
    taps = jnp.concatenate(
        [
            jnp.swapaxes(conv_taps[:, :main].reshape(3, tiles, tile), 0, 1),
            jnp.pad(conv_taps[:, main:], ((0, 0), (spot, tile - spot - spare)))[None],
        ],
        axis=0,
    )

    pay, rows, cols_aux = pl.pallas_call(
        state_kernel,
        out_shape=(
            shape((DH + 16, width), BF16),
            shape((8, tokens), F32),
            shape((tokens, 8), F32),
        ),
        scratch_shapes=[pltpu.VMEM((8, tokens), F32)],
        name="state",
    )(keys, values, in_gate, forget, doc_ids.reshape(1, tokens))
    count = lax.axis_size(SP)
    reach = -(-(DOC_MAX - 1) // tokens)
    pays = [
        lax.ppermute(pay, SP, [(i, i + k) for i in range(count - k)]) for k in range(1, reach + 1)
    ]
    local = pl.pallas_call(
        local_kernel,
        out_shape=shape((tokens, width), F32),
        name="local",
    )(query, keys, values, rows, cols_aux)
    chip, core = lax.axis_index("y"), lax.axis_index("c")
    ring, cores = lax.axis_size("y"), lax.axis_size("c")
    order = (chip + jnp.array([2, 2, 1, 1, 3, 3, 0, 0], jnp.int32)) % ring * cores + (
        core ^ jnp.array([1, 0] * ring, jnp.int32)
    )
    swap, own, near, far_flags = pl.pallas_call(
        mix_kernel,
        grid_spec=pltpu.PrefetchScalarGridSpec(
            num_scalar_prefetch=1,
            grid=(ring,),
            in_specs=[
                whole((tokens, width)),
                whole((tokens, width)),
                whole((tokens, width)),
                whole((8, tokens)),
                whole((tokens, 8)),
                whole((1, width)),
                pl.BlockSpec((width, cols), lambda j, order: (0, order[2 * j])),
                pl.BlockSpec((width, cols), lambda j, order: (0, order[2 * j + 1])),
                *[whole((DH + 16, width)) for _ in pays],
            ],
            out_specs=(
                pl.BlockSpec((1, tokens, cols), lambda j, order: (j, 0, 0)),
                pl.BlockSpec((1, tokens, cols), lambda j, order: (j, 0, 0)),
                whole((tokens, 128)),
                whole((tokens, 128)),
            ),
            scratch_shapes=[pltpu.VMEM((tokens, width), BF16)],
        ),
        out_shape=(
            shape((ring, tokens, cols), BF16),
            shape((ring, tokens, cols), BF16),
            shape((tokens, 128), F32),
            shape((tokens, 128), F32),
        ),
        name="mix",
    )(order, query, out_gate, local, rows, cols_aux, head_gain.reshape(1, width), w_out, w_out, *pays)
    attended = summed_over_tp(
        swap[:3],
        own[0],
        lambda other: tuple(added(own[k], other[k]).astype(BF16) for k in (1, 2)),
        lambda: (swap[3], own[3]),
    )
    residual_own = resid.astype(F32) + jnp.concatenate(attended, axis=0)
    pieces = gathered_over_tp(residual_own.astype(BF16))
    places = (chip + jnp.array([0, ring - 1, 1, 2] * 2, jnp.int32)) % ring * cores + (
        core ^ jnp.array([0] * ring + [1] * ring, jnp.int32)
    )
    block = 96
    normed, send = pl.pallas_call(
        norm_kernel,
        grid_spec=pltpu.PrefetchScalarGridSpec(
            num_scalar_prefetch=1,
            grid=(tokens // block,),
            in_specs=[
                *[pl.BlockSpec((block, cols), lambda i, places: (i, 0)) for _ in pieces],
                whole((1, model)),
            ],
            out_specs=(whole((tokens + HALO, model)), whole((HALO, model))),
        ),
        out_shape=(shape((tokens + HALO, model), BF16), shape((HALO, model), BF16)),
        compiler_params=pltpu.CompilerParams(vmem_limit_bytes=40 * 2**20),
        name="norm",
    )(places, *pieces, ffn_gain.reshape(1, model))
    edge = lax.ppermute(send, SP, [(i, i + 1) for i in range(count - 1)])
    normed = lax.dynamic_update_slice(normed, edge, (0, 0))
    tail_at = 3 * main // 128
    order = (chip + jnp.array([2, 2, 1, 3, 1, 3, 0, 0], jnp.int32)) % ring * cores + (
        core ^ jnp.array([1, 0, 1, 1, 0, 0, 1, 0], jnp.int32)
    )
    hidden, swap, own = pl.pallas_call(
        mixer_kernel,
        grid_spec=pltpu.PrefetchScalarGridSpec(
            num_scalar_prefetch=1,
            grid=(tiles + 2,),
            in_specs=[
                pl.BlockSpec(
                    (tokens + HALO, model), lambda j, order: (0, 0), pipeline_mode=pl.Buffered(1)
                ),
                whole((tokens, 128)),
                whole((tokens, 128)),
                whole((tiles + 1, 3, tile)),
                pl.BlockSpec((model, tile), lambda j, order: (0, jnp.minimum(j, tiles - 1))),
                pl.BlockSpec(
                    (model, tile), lambda j, order: (0, tiles + jnp.minimum(j, tiles - 1))
                ),
                pl.BlockSpec(
                    (model, 128), lambda j, order: (0, tail_at), pipeline_mode=pl.Buffered(1)
                ),
                pl.BlockSpec(memory_space=pl.ANY),
            ],
            out_specs=(
                whole((tokens, main + 128)),
                whole((3, tokens, cols)),
                whole((1, tokens, cols)),
            ),
            scratch_shapes=[
                pltpu.VMEM((2, tokens + HALO, tile), F32),
                pltpu.VMEM((2, tokens + HALO, tile), F32),
                pltpu.VMEM((tokens + HALO, 128), F32),
                pltpu.VMEM((2, 2 * cols, main + 128), BF16),
                pltpu.SemaphoreType.DMA((8,)),
            ],
        ),
        out_shape=(
            shape((tokens, main + 128), BF16),
            shape((3, tokens, cols), BF16),
            shape((1, tokens, cols), BF16),
        ),
        compiler_params=pltpu.CompilerParams(vmem_limit_bytes=58 * 2**20),
        name="mixer",
    )(order, normed, near, far_flags, taps, *[weights] * 4)

    def more(kernel, at, given, specs):
        def spot(k, col):
            return lambda j, order: (order[at + k], col)

        one = shape((tokens, cols), BF16)
        return pl.pallas_call(
            kernel,
            grid_spec=pltpu.PrefetchScalarGridSpec(
                num_scalar_prefetch=1,
                grid=(1,),
                in_specs=[
                    whole((tokens, main + 128)),
                    pl.BlockSpec((cols, main), spot(0, 2)),
                    pl.BlockSpec((cols, main), spot(1, 2)),
                    pl.BlockSpec((cols, 128), spot(0, tail_at)),
                    pl.BlockSpec((cols, 128), spot(1, tail_at)),
                    *specs,
                ],
                out_specs=(whole((tokens, cols)), whole((tokens, cols))),
            ),
            out_shape=(one, one),
            compiler_params=pltpu.CompilerParams(vmem_limit_bytes=40 * 2**20),
        )(order, hidden, *[weights] * 4, *given)

    down = summed_over_tp(
        swap,
        own[0],
        lambda other: more(
            side_kernel,
            4,
            (other, other),
            [pl.BlockSpec((1, tokens, cols), lambda j, order, k=k: (k, 0, 0)) for k in (1, 2)],
        ),
        lambda: more(down_kernel, 6, (), []),
    )
    return (residual_own + jnp.concatenate(down, axis=0)).astype(BF16)


def solution(mesh):
    torus = Mesh(mesh.devices.reshape(4, 4, 4, 2), ("z", "x", "y", "c"))
    placed = (
        P(SP, TP),
        P(SP, TP),
        P(SP, TP),
        P(SP, TP),
        P(SP, TP),
        P(TP, SP),
        P(TP, SP),
        P(SP),
        P(TP),
        P(TP, None),
        P(),
        P(SP, TP),
        P(SP, TP),
        P(None, TP),
        P(TP, SP),
    )
    return jax.shard_map(layer, mesh=torus, in_specs=placed, out_specs=P(SP, TP), check_vma=False)
```

profile of v0, /device:TPU:0, one launch (start us, length us, event | category | flops | bytes accessed | tf_op | source)
XLA Modules:
  0.0 209.4 jit_solution(15804141036714992904)
XLA Ops:
  6.5 2.5 %pack.1 = bf16[192,3200]{1,0:T(8,128)(2,1)} custom-call(bf16[192,1056]{1,0:T(8,128)(2,1)} %gate_ref.2, bf16[192,1056]{1,0:T(8,128)(2,1)} %value_ref.1, bf16[192,1056]{1,0:T(8,128)(2,1)} %bitcast.36), custom_call_target="tpu_custom_call" | custom-call | tf_op jit(solution)/shard_map/pack/pallas_call | solution.py:437
  9.1 0.9 copy-done.5
  10.0 0.9 copy.25.k_ref
  10.9 0.9 copy.26.v_ref
  12.4 3.6 %state.1 = (bf16[112,192]{1,0:T(8,128)(2,1)}, f32[8,768]{1,0:T(8,128)}, f32[768,8]{1,0:T(8,128)}) custom-call(bf16[768,192]{1,0:T(8,128)(2,1)} %copy.25.k_ref, bf16[768,192]{1,0:T(8,128)(2,1)} %copy.26.v_ref, f32[2,768]{1,0:T(2,128)} %in_ref.1, f32[2,768]{1,0:T(2,128)} %forget_ref.1, s32[1,768]{1,0:T(1,128)} %reshape.42.doc_ref), custom_call_target="tpu_custom_call" | custom-call | tf_op jit(solution)/shard_map/state/pallas_call | solution.py:454
  16.1 3.5 %collective-permute-start = (bf16[112,192]{1,0:T(8,128)(2,1)}, bf16[112,192]{1,0:T(8,128)(2,1)S(1)}, u32[]{:S(2)}, u32[]{:S(2)}) collective-permute-start(bf16[112,192]{1,0:T(8,128)(2,1)} %get-tuple-element.23), channel_id=1, source_target_pairs={{0,8},{8,16},{16,24},{24,32},{32,40},{40,48},{48,56},{56,64},{64,7... | collective-permute-start | bytes 129032 | tf_op jit(solution)/shard_map/ppermute | solution.py:467
  19.6 4.6 %collective-permute-start.1 = (bf16[112,192]{1,0:T(8,128)(2,1)}, bf16[112,192]{1,0:T(8,128)(2,1)S(1)}, u32[]{:S(2)}, u32[]{:S(2)}) collective-permute-start(bf16[112,192]{1,0:T(8,128)(2,1)} %get-tuple-element.23), channel_id=1, source_target_pairs={{0,16},{8,24},{16,32},{24,40},{32,48},{40,56},{48,64},{56,72},{64,... | collective-permute-start | bytes 129032 | tf_op jit(solution)/shard_map/ppermute | solution.py:467
  24.2 4.7 %collective-permute-start.2 = (bf16[112,192]{1,0:T(8,128)(2,1)}, bf16[112,192]{1,0:T(8,128)(2,1)S(1)}, u32[]{:S(2)}, u32[]{:S(2)}) collective-permute-start(bf16[112,192]{1,0:T(8,128)(2,1)} %get-tuple-element.23), channel_id=1, source_target_pairs={{0,24},{8,32},{16,40},{24,48},{32,56},{40,64},{48,72},{56,80},{64,... | collective-permute-start | bytes 129032 | tf_op jit(solution)/shard_map/ppermute | solution.py:467
  28.9 3.8 %collective-permute-start.3 = (bf16[112,192]{1,0:T(8,128)(2,1)}, bf16[112,192]{1,0:T(8,128)(2,1)S(1)}, u32[]{:S(2)}, u32[]{:S(2)}) collective-permute-start(bf16[112,192]{1,0:T(8,128)(2,1)} %get-tuple-element.23), channel_id=1, source_target_pairs={{0,32},{8,40},{16,48},{24,56},{32,64},{40,72},{48,80},{56,88},{64,... | collective-permute-start | bytes 129032 | tf_op jit(solution)/shard_map/ppermute | solution.py:467
  33.3 0.9 copy.27.q_ref
  34.2 0.9 copy.28.gate_ref
  35.2 3.7 %local.1.local_ref = f32[768,192]{1,0:T(8,128)} custom-call(bf16[768,192]{1,0:T(8,128)(2,1)} %copy.27.q_ref, bf16[768,192]{1,0:T(8,128)(2,1)} %copy.25.k_ref, bf16[768,192]{1,0:T(8,128)(2,1)} %copy.26.v_ref, f32[8,768]{1,0:T(8,128)} %get-tuple-element.21.row_ref, f32[768,8]{1,0:T(8,128)} %get-tuple-element.22.col_ref), custom_call_target="tpu_custom_call" | custom-call | tf_op jit(solution)/shard_map/local/pallas_call | solution.py:469
  39.5 8.0 %mix.1 = (bf16[4,768,384]{2,1,0:T(8,128)(2,1)}, bf16[4,768,384]{2,1,0:T(8,128)(2,1)}, f32[768,128]{1,0:T(8,128)}, f32[768,128]{1,0:T(8,128)}) custom-call(s32[8]{0:T(128)} %fusion.10.order_ref, bf16[768,192]{1,0:T(8,128)(2,1)} %copy.27.q_ref, bf16[768,192]{1,0:T(8,128)(2,1)} %copy.28.gate_ref, f32[768,192]{1,0:T(8,128)} %local.1.local_ref, ...), custom_call_target="tpu_custom_call" | custom-call | tf_op jit(solution)/shard_map/mix/pallas_call | solution.py:479
  47.5 1.8 slice.114
  49.4 1.1 slice_bitcast_fusion
  51.1 2.0 collective-permute-done.5
  53.6 3.1 %collective-permute-start.10 = (bf16[384,384]{1,0:T(8,128)(2,1)S(1)}, bf16[384,384]{1,0:T(8,128)(2,1)S(1)}, u32[]{:S(2)}, u32[]{:S(2)}) collective-permute-start(bf16[384,384]{1,0:T(8,128)(2,1)S(1)} %get-tuple-element.47), channel_id=1, source_target_pairs={{0,6},{2,0},{4,2},{6,4},{1,7},{3,1},{5,3},{7,5},{8,14},{10,8},{12,... | collective-permute-start | bytes 884744 | tf_op jit(solution)/shard_map/ppermute | solution.py:376
  56.7 3.3 %collective-permute-start.8 = (bf16[384,384]{1,0:T(8,128)(2,1)S(1)}, bf16[384,384]{1,0:T(8,128)(2,1)S(1)}, u32[]{:S(2)}, u32[]{:S(2)}) collective-permute-start(bf16[384,384]{1,0:T(8,128)(2,1)S(1)} %slice_bitcast_fusion.6), channel_id=1, source_target_pairs={{0,6},{2,0},{4,2},{6,4},{1,7},{3,1},{5,3},{7,5},{8,14},{10,8},{12,... | collective-permute-start | bytes 884744 | tf_op jit(solution)/shard_map/ppermute | solution.py:376
  60.1 3.9 %collective-permute-done.10 = bf16[384,384]{1,0:T(8,128)(2,1)S(1)} collective-permute-done((bf16[384,384]{1,0:T(8,128)(2,1)S(1)}, bf16[384,384]{1,0:T(8,128)(2,1)S(1)}, u32[]{:S(2)}, u32[]{:S(2)}) %collective-permute-start.10) | collective-permute-done | bytes 294944 | tf_op jit(solution)/shard_map/ppermute | solution.py:376
  64.1 3.8 %collective-permute-start.11 = (bf16[384,384]{1,0:T(8,128)(2,1)S(1)}, bf16[384,384]{1,0:T(8,128)(2,1)S(1)}, u32[]{:S(2)}, u32[]{:S(2)}) collective-permute-start(bf16[384,384]{1,0:T(8,128)(2,1)S(1)} %fusion.6), channel_id=1, source_target_pairs={{0,6},{2,0},{4,2},{6,4},{1,7},{3,1},{5,3},{7,5},{8,14},{10,8},{12,... | collective-permute-start | bytes 884744 | tf_op jit(solution)/shard_map/ppermute | solution.py:376
  68.2 2.2 %collective-permute-done.8 = bf16[384,384]{1,0:T(8,128)(2,1)S(1)} collective-permute-done((bf16[384,384]{1,0:T(8,128)(2,1)S(1)}, bf16[384,384]{1,0:T(8,128)(2,1)S(1)}, u32[]{:S(2)}, u32[]{:S(2)}) %collective-permute-start.8) | collective-permute-done | bytes 294944 | tf_op jit(solution)/shard_map/ppermute | solution.py:376
  70.3 3.7 %collective-permute-done.9 = bf16[384,384]{1,0:T(8,128)(2,1)S(1)} collective-permute-done((bf16[384,384]{1,0:T(8,128)(2,1)S(1)}, bf16[384,384]{1,0:T(8,128)(2,1)S(1)}, u32[]{:S(2)}, u32[]{:S(2)}) %collective-permute-start.9) | collective-permute-done | bytes 294944 | tf_op jit(solution)/shard_map/ppermute | solution.py:376
  74.0 1.8 collective-permute-done.11
  75.8 3.4 %collective-permute-done.7 = bf16[384,384]{1,0:T(8,128)(2,1)S(1)} collective-permute-done((bf16[384,384]{1,0:T(8,128)(2,1)S(1)}, bf16[384,384]{1,0:T(8,128)(2,1)S(1)}, u32[]{:S(2)}, u32[]{:S(2)}) %collective-permute-start.7) | collective-permute-done | bytes 294944 | tf_op jit(solution)/shard_map/ppermute | solution.py:376
  79.7 3.2 %collective-permute-start.13 = (bf16[768,384]{1,0:T(8,128)(2,1)S(1)}, bf16[768,384]{1,0:T(8,128)(2,1)S(1)}, u32[]{:S(2)}, u32[]{:S(2)}) collective-permute-start(bf16[768,384]{1,0:T(8,128)(2,1)S(1)} %fusion.1.refs_0_), channel_id=1, source_target_pairs={{0,6},{2,0},{4,2},{6,4},{1,7},{3,1},{5,3},{7,5},{8,14},{10,8},{12,... | collective-permute-start | bytes 1769480 | tf_op jit(solution)/shard_map/ppermute | solution.py:376
  83.0 12.3 %collective-permute-done.12.refs_1_ = bf16[768,384]{1,0:T(8,128)(2,1)S(1)} collective-permute-done((bf16[768,384]{1,0:T(8,128)(2,1)S(1)}, bf16[768,384]{1,0:T(8,128)(2,1)S(1)}, u32[]{:S(2)}, u32[]{:S(2)}) %collective-permute-start.12) | collective-permute-done | bytes 589856 | tf_op jit(solution)/shard_map/ppermute | solution.py:376
  95.4 3.3 %collective-permute-start.15 = (bf16[384,384]{1,0:T(8,128)(2,1)S(1)}, bf16[384,384]{1,0:T(8,128)(2,1)S(1)}, u32[]{:S(2)}, u32[]{:S(2)}) collective-permute-start(bf16[384,384]{1,0:T(8,128)(2,1)S(1)} %slice.158), channel_id=1, source_target_pairs={{0,6},{2,0},{4,2},{6,4},{1,7},{3,1},{5,3},{7,5},{8,14},{10,8},{12,... | collective-permute-start | bytes 884744 | tf_op jit(solution)/shard_map/ppermute | solution.py:376
  99.2 4.6 %collective-permute-done.14 = bf16[384,384]{1,0:T(8,128)(2,1)S(1)} collective-permute-done((bf16[384,384]{1,0:T(8,128)(2,1)S(1)}, bf16[384,384]{1,0:T(8,128)(2,1)S(1)}, u32[]{:S(2)}, u32[]{:S(2)}) %collective-permute-start.14) | collective-permute-done | bytes 294944 | tf_op jit(solution)/shard_map/ppermute | solution.py:376
  104.7 1.3 collective-permute-done.19.refs_7_
  106.0 5.3 %norm.1 = (bf16[784,3072]{1,0:T(8,128)(2,1)}, bf16[16,3072]{1,0:T(8,128)(2,1)S(1)}) custom-call(s32[8]{0:T(128)S(1)} %fusion.16.order_ref, bf16[768,384]{1,0:T(8,128)(2,1)S(1)} %fusion.1.refs_0_, bf16[768,384]{1,0:T(8,128)(2,1)S(1)} %collective-permute-done.12.refs_1_, bf16[768,384]{1,0:T(8,128)(2,1)S(1)} %collective-permute-done.13.refs_2_, ...), custom_call_target="tpu_custom_call" | custom-call | tf_op jit(solution)/shard_map/norm/pallas_call | solution.py:523
  111.4 2.4 %collective-permute-start.20 = (bf16[16,3072]{1,0:T(8,128)(2,1)S(1)}, bf16[16,3072]{1,0:T(8,128)(2,1)S(1)}, u32[]{:S(2)}, u32[]{:S(2)}) collective-permute-start(bf16[16,3072]{1,0:T(8,128)(2,1)S(1)} %get-tuple-element.27), channel_id=1, source_target_pairs={{0,8},{8,16},{16,24},{24,32},{32,40},{40,48},{48,56},{56,64},{64,7... | collective-permute-start | bytes 294920 | tf_op jit(solution)/shard_map/ppermute | solution.py:538
  113.8 0.6 pad_maximum_fusion.taps_ref
  114.4 4.4 %collective-permute-done.20 = bf16[16,3072]{1,0:T(8,128)(2,1)S(1)} collective-permute-done((bf16[16,3072]{1,0:T(8,128)(2,1)S(1)}, bf16[16,3072]{1,0:T(8,128)(2,1)S(1)}, u32[]{:S(2)}, u32[]{:S(2)}) %collective-permute-start.20) | collective-permute-done | bytes 98336 | tf_op jit(solution)/shard_map/ppermute | solution.py:538
  118.8 0.6 constant_dynamic-update-slice_fusion.2.x_ref
  119.5 22.1 %all-gather.2.cloned.1.call-done.wg_ref.wv_ref.wt_ref.w_ref.wa_ref.wb_ref.ta_ref.tb_ref = bf16[3072,3200]{1,0:T(8,128)(2,1)} async-done(((bf16[192,3200]{1,0:T(8,128)(2,1)}), bf16[3072,3200]{1,0:T(8,128)(2,1)}) %all-gather.2.cloned.1.call-update) | async-done | bytes 19660816 | tf_op jit(solution)/shard_map/all_gather | solution.py:442
  141.6 24.1 %mixer.1 = (bf16[768,1152]{1,0:T(8,128)(2,1)}, bf16[3,768,384]{2,1,0:T(8,128)(2,1)}, bf16[1,768,384]{2,1,0:T(8,128)(2,1)}) custom-call(s32[8]{0:T(128)} %fusion.13.order_ref, bf16[784,3072]{1,0:T(8,128)(2,1)} %constant_dynamic-update-slice_fusion.2.x_ref, f32[768,128]{1,0:T(8,128)} %get-tuple-element.28.near_ref, f32[768,128]{1,0:T(8,128)} %get-tuple-element.29.far_ref, ...), custom_call_target="tpu_custom_call" | custom-call | tf_op jit(solution)/shard_map/mixer/pallas_call | solution.py:544
  165.8 3.9 %collective-permute-done.22.a_ref.b_ref = bf16[3,768,384]{2,1,0:T(8,128)(2,1)S(1)} collective-permute-done((bf16[3,768,384]{2,1,0:T(8,128)(2,1)}, bf16[3,768,384]{2,1,0:T(8,128)(2,1)S(1)}, u32[]{:S(2)}, u32[]{:S(2)}) %collective-permute-start.22) | collective-permute-done | bytes 1769504 | tf_op jit(solution)/shard_map/ppermute | solution.py:380
  169.6 1.3 add_convert_fusion
  171.1 3.0 %collective-permute-start.27 = (bf16[384,384]{1,0:T(8,128)(2,1)S(1)}, bf16[384,384]{1,0:T(8,128)(2,1)S(1)}, u32[]{:S(2)}, u32[]{:S(2)}) collective-permute-start(bf16[384,384]{1,0:T(8,128)(2,1)S(1)} %get-tuple-element.45), channel_id=1, source_target_pairs={{0,6},{2,0},{4,2},{6,4},{1,7},{3,1},{5,3},{7,5},{8,14},{10,8},{12,... | collective-permute-start | bytes 884744 | tf_op jit(solution)/shard_map/ppermute | solution.py:376
  174.1 3.7 %shard_map.199 = (bf16[768,384]{1,0:T(8,128)(2,1)S(1)}, bf16[768,384]{1,0:T(8,128)(2,1)S(1)}) custom-call(s32[8]{0:T(128)S(1)} %copy-done.2, bf16[768,1152]{1,0:T(8,128)(2,1)S(1)} %copy-done, bf16[3072,3200]{1,0:T(8,128)(2,1)} %all-gather.2.cloned.1.call-done.wg_ref.wv_ref.wt_ref.w_ref.wa_ref.wb_ref.ta_ref.tb_ref, ...), custom_call_target="tpu_custom_call" | custom-call | tf_op jit(solution)/shard_map/pallas_call | solution.py:592
  177.9 3.7 %shard_map.200 = (bf16[768,384]{1,0:T(8,128)(2,1)S(1)}, bf16[768,384]{1,0:T(8,128)(2,1)S(1)}) custom-call(s32[8]{0:T(128)S(1)} %copy-done.2, bf16[768,1152]{1,0:T(8,128)(2,1)S(1)} %copy-done, bf16[3072,3200]{1,0:T(8,128)(2,1)} %all-gather.2.cloned.1.call-done.wg_ref.wv_ref.wt_ref.w_ref.wa_ref.wb_ref.ta_ref.tb_ref, ...), custom_call_target="tpu_custom_call" | custom-call | tf_op jit(solution)/shard_map/pallas_call | solution.py:592
  181.6 3.3 %collective-permute-start.25 = (bf16[384,384]{1,0:T(8,128)(2,1)S(1)}, bf16[384,384]{1,0:T(8,128)(2,1)S(1)}, u32[]{:S(2)}, u32[]{:S(2)}) collective-permute-start(bf16[384,384]{1,0:T(8,128)(2,1)S(1)} %slice.140), channel_id=1, source_target_pairs={{0,6},{2,0},{4,2},{6,4},{1,7},{3,1},{5,3},{7,5},{8,14},{10,8},{12,... | collective-permute-start | bytes 884744 | tf_op jit(solution)/shard_map/ppermute | solution.py:376
  185.1 3.3 %collective-permute-start.28 = (bf16[384,384]{1,0:T(8,128)(2,1)S(1)}, bf16[384,384]{1,0:T(8,128)(2,1)S(1)}, u32[]{:S(2)}, u32[]{:S(2)}) collective-permute-start(bf16[384,384]{1,0:T(8,128)(2,1)S(1)} %add_convert_fusion.4), channel_id=1, source_target_pairs={{0,6},{2,0},{4,2},{6,4},{1,7},{3,1},{5,3},{7,5},{8,14},{10,8},{12,... | collective-permute-start | bytes 884744 | tf_op jit(solution)/shard_map/ppermute | solution.py:376
  188.8 3.6 %collective-permute-done.25 = bf16[384,384]{1,0:T(8,128)(2,1)S(1)} collective-permute-done((bf16[384,384]{1,0:T(8,128)(2,1)S(1)}, bf16[384,384]{1,0:T(8,128)(2,1)S(1)}, u32[]{:S(2)}, u32[]{:S(2)}) %collective-permute-start.25) | collective-permute-done | bytes 294944 | tf_op jit(solution)/shard_map/ppermute | solution.py:376
  192.3 3.8 %collective-permute-done.26 = bf16[384,384]{1,0:T(8,128)(2,1)S(1)} collective-permute-done((bf16[384,384]{1,0:T(8,128)(2,1)S(1)}, bf16[384,384]{1,0:T(8,128)(2,1)S(1)}, u32[]{:S(2)}, u32[]{:S(2)}) %collective-permute-start.26) | collective-permute-done | bytes 294944 | tf_op jit(solution)/shard_map/ppermute | solution.py:376
  196.1 1.7 collective-permute-done.28
  197.8 3.5 %collective-permute-done.24 = bf16[384,384]{1,0:T(8,128)(2,1)S(1)} collective-permute-done((bf16[384,384]{1,0:T(8,128)(2,1)S(1)}, bf16[384,384]{1,0:T(8,128)(2,1)S(1)}, u32[]{:S(2)}, u32[]{:S(2)}) %collective-permute-start.24) | collective-permute-done | bytes 294944 | tf_op jit(solution)/shard_map/ppermute | solution.py:376
  201.5 1.0 fusion
  (100 shorter events, 6.3 us)
Async XLA Ops:
  6.5 135.1 %all-gather.2.cloned.1.call-start = ((), (), s32[]{:S(2)}) async-start(), calls=%async_computation | async-start | bytes 20889600 | tf_op jit(solution)/shard_map/all_gather | solution.py:442
  9.0 1.0 copy-start.5
  9.0 1.9 copy-start.6
  9.0 2.8 %copy-start.13 = (s32[768]{0:T(1024)S(1)}, s32[768]{0:T(1024)}, u32[]{:S(2)}) copy-start(s32[768]{0:T(1024)} %param.28) | copy-start | bytes 9220
  10.0 22.7 %copy-start.18 = (s32[8]{0:T(128)S(1)}, s32[8]{0:T(128)}, u32[]{:S(2)}) copy-start(s32[8]{0:T(128)} %constant.50.clone) | copy-start | bytes 100
  10.0 22.8 %copy-start.19 = (s32[8]{0:T(128)S(1)}, s32[8]{0:T(128)}, u32[]{:S(2)}) copy-start(s32[8]{0:T(128)} %constant.51.clone) | copy-start | bytes 100
  10.0 23.3 %copy-start.7 = (bf16[768,192]{0,1:T(8,128)(2,1)S(1)}, bf16[768,192]{0,1:T(8,128)(2,1)}, u32[]{:S(2)}) copy-start(bf16[768,192]{0,1:T(8,128)(2,1)} %param.22) | copy-start | bytes 884740
  10.9 23.3 %copy-start.8 = (bf16[768,192]{0,1:T(8,128)(2,1)S(1)}, bf16[768,192]{0,1:T(8,128)(2,1)}, u32[]{:S(2)}) copy-start(bf16[768,192]{0,1:T(8,128)(2,1)} %param.25) | copy-start | bytes 884740
  16.1 22.8 %collective-permute-start = (bf16[112,192]{1,0:T(8,128)(2,1)}, bf16[112,192]{1,0:T(8,128)(2,1)S(1)}, u32[]{:S(2)}, u32[]{:S(2)}) collective-permute-start(bf16[112,192]{1,0:T(8,128)(2,1)} %get-tuple-element.23), channel_id=1, source_target_pairs={{0,8},{8,16},{16,24},{24,32},{32,40},{40,48},{48,56},{56,64},{64,7... | collective-permute-start | bytes 129032 | tf_op jit(solution)/shard_map/ppermute | solution.py:467
  19.6 19.3 %collective-permute-start.1 = (bf16[112,192]{1,0:T(8,128)(2,1)}, bf16[112,192]{1,0:T(8,128)(2,1)S(1)}, u32[]{:S(2)}, u32[]{:S(2)}) collective-permute-start(bf16[112,192]{1,0:T(8,128)(2,1)} %get-tuple-element.23), channel_id=1, source_target_pairs={{0,16},{8,24},{16,32},{24,40},{32,48},{40,56},{48,64},{56,72},{64,... | collective-permute-start | bytes 129032 | tf_op jit(solution)/shard_map/ppermute | solution.py:467
  24.2 14.6 %collective-permute-start.2 = (bf16[112,192]{1,0:T(8,128)(2,1)}, bf16[112,192]{1,0:T(8,128)(2,1)S(1)}, u32[]{:S(2)}, u32[]{:S(2)}) collective-permute-start(bf16[112,192]{1,0:T(8,128)(2,1)} %get-tuple-element.23), channel_id=1, source_target_pairs={{0,24},{8,32},{16,40},{24,48},{32,56},{40,64},{48,72},{56,80},{64,... | collective-permute-start | bytes 129032 | tf_op jit(solution)/shard_map/ppermute | solution.py:467
  28.9 10.0 %collective-permute-start.3 = (bf16[112,192]{1,0:T(8,128)(2,1)}, bf16[112,192]{1,0:T(8,128)(2,1)S(1)}, u32[]{:S(2)}, u32[]{:S(2)}) collective-permute-start(bf16[112,192]{1,0:T(8,128)(2,1)} %get-tuple-element.23), channel_id=1, source_target_pairs={{0,32},{8,40},{16,48},{24,56},{32,64},{40,72},{48,80},{56,88},{64,... | collective-permute-start | bytes 129032 | tf_op jit(solution)/shard_map/ppermute | solution.py:467
  47.5 5.6 %copy-start.4 = (bf16[4,768,384]{2,1,0:T(8,128)(2,1)S(1)}, bf16[4,768,384]{2,1,0:T(8,128)(2,1)}, u32[]{:S(2)}) copy-start(bf16[4,768,384]{2,1,0:T(8,128)(2,1)} %get-tuple-element.24) | copy-start | bytes 7077892
  49.3 3.8 %collective-permute-start.5 = (bf16[3,768,384]{2,1,0:T(8,128)(2,1)S(1)}, bf16[3,768,384]{2,1,0:T(8,128)(2,1)S(1)}, u32[]{:S(2)}, u32[]{:S(2)}) collective-permute-start(bf16[3,768,384]{2,1,0:T(8,128)(2,1)S(1)} %slice.114), channel_id=1, source_target_pairs={{0,1},{1,0},{2,3},{3,2},{4,5},{5,4},{6,7},{7,6},{8,9},{9,8},{10,11... | collective-permute-start | bytes 5308424 | tf_op jit(solution)/shard_map/ppermute | solution.py:380
  50.5 17.5 %collective-permute-start.4 = (bf16[768,384]{1,0:T(8,128)(2,1)S(1)}, bf16[768,384]{1,0:T(8,128)(2,1)S(1)}, u32[]{:S(2)}, u32[]{:S(2)}) collective-permute-start(bf16[768,384]{1,0:T(8,128)(2,1)S(1)} %slice_bitcast_fusion), channel_id=1, source_target_pairs={{0,1},{1,0},{2,3},{3,2},{4,5},{5,4},{6,7},{7,6},{8,9},{9,8},{10,11... | collective-permute-start | bytes 1769480 | tf_op jit(solution)/shard_map/ppermute | solution.py:380
  53.6 10.4 %collective-permute-start.10 = (bf16[384,384]{1,0:T(8,128)(2,1)S(1)}, bf16[384,384]{1,0:T(8,128)(2,1)S(1)}, u32[]{:S(2)}, u32[]{:S(2)}) collective-permute-start(bf16[384,384]{1,0:T(8,128)(2,1)S(1)} %get-tuple-element.47), channel_id=1, source_target_pairs={{0,6},{2,0},{4,2},{6,4},{1,7},{3,1},{5,3},{7,5},{8,14},{10,8},{12,... | collective-permute-start | bytes 884744 | tf_op jit(solution)/shard_map/ppermute | solution.py:376
  56.6 11.2 %collective-permute-start.6 = (bf16[384,384]{1,0:T(8,128)(2,1)S(1)}, bf16[384,384]{1,0:T(8,128)(2,1)S(1)}, u32[]{:S(2)}, u32[]{:S(2)}) collective-permute-start(bf16[384,384]{1,0:T(8,128)(2,1)S(1)} %get-tuple-element.46), channel_id=1, source_target_pairs={{0,2},{2,4},{4,6},{6,0},{1,3},{3,5},{5,7},{7,1},{8,10},{10,12},{12... | collective-permute-start | bytes 884744 | tf_op jit(solution)/shard_map/ppermute | solution.py:376
  56.7 13.7 %collective-permute-start.8 = (bf16[384,384]{1,0:T(8,128)(2,1)S(1)}, bf16[384,384]{1,0:T(8,128)(2,1)S(1)}, u32[]{:S(2)}, u32[]{:S(2)}) collective-permute-start(bf16[384,384]{1,0:T(8,128)(2,1)S(1)} %slice_bitcast_fusion.6), channel_id=1, source_target_pairs={{0,6},{2,0},{4,2},{6,4},{1,7},{3,1},{5,3},{7,5},{8,14},{10,8},{12,... | collective-permute-start | bytes 884744 | tf_op jit(solution)/shard_map/ppermute | solution.py:376
  60.0 14.0 %collective-permute-start.9 = (bf16[384,384]{1,0:T(8,128)(2,1)S(1)}, bf16[384,384]{1,0:T(8,128)(2,1)S(1)}, u32[]{:S(2)}, u32[]{:S(2)}) collective-permute-start(bf16[384,384]{1,0:T(8,128)(2,1)S(1)} %slice_bitcast_fusion.5), channel_id=1, source_target_pairs={{0,2},{2,4},{4,6},{6,0},{1,3},{3,5},{5,7},{7,1},{8,10},{10,12},{12... | collective-permute-start | bytes 884744 | tf_op jit(solution)/shard_map/ppermute | solution.py:376
  64.1 11.7 %collective-permute-start.11 = (bf16[384,384]{1,0:T(8,128)(2,1)S(1)}, bf16[384,384]{1,0:T(8,128)(2,1)S(1)}, u32[]{:S(2)}, u32[]{:S(2)}) collective-permute-start(bf16[384,384]{1,0:T(8,128)(2,1)S(1)} %fusion.6), channel_id=1, source_target_pairs={{0,6},{2,0},{4,2},{6,4},{1,7},{3,1},{5,3},{7,5},{8,14},{10,8},{12,... | collective-permute-start | bytes 884744 | tf_op jit(solution)/shard_map/ppermute | solution.py:376
  67.9 11.3 %collective-permute-start.7 = (bf16[384,384]{1,0:T(8,128)(2,1)S(1)}, bf16[384,384]{1,0:T(8,128)(2,1)S(1)}, u32[]{:S(2)}, u32[]{:S(2)}) collective-permute-start(bf16[384,384]{1,0:T(8,128)(2,1)S(1)} %fusion.7), channel_id=1, source_target_pairs={{0,2},{2,4},{4,6},{6,0},{1,3},{3,5},{5,7},{7,1},{8,10},{10,12},{12... | collective-permute-start | bytes 884744 | tf_op jit(solution)/shard_map/ppermute | solution.py:376
  68.2 11.3 %copy-start.3 = (bf16[768,384]{1,0:T(8,128)(2,1)S(1)}, bf16[768,384]{1,0:T(8,128)(2,1)}, u32[]{:S(2)}) copy-start(bf16[768,384]{1,0:T(8,128)(2,1)} %param.21) | copy-start | bytes 1769476
  79.6 24.5 %slice-start.1 = ((f32[3,1056]{1,0:T(4,128)}), f32[3,32]{1,0:T(4,128)S(1)}, s32[]{:S(2)}) async-start(f32[3,1056]{1,0:T(4,128)} %param.34), calls=%async_computation.2 | async-start | bytes 4096 | tf_op jit(solution)/shard_map/slice | solution.py:449
  79.6 24.5 %copy-start.16 = (s32[8]{0:T(128)S(1)}, s32[8]{0:T(128)}, u32[]{:S(2)}) copy-start(s32[8]{0:T(128)} %constant.52.clone) | copy-start | bytes 100
  79.6 24.5 %copy-start.17 = (s32[8]{0:T(128)S(1)}, s32[8]{0:T(128)}, u32[]{:S(2)}) copy-start(s32[8]{0:T(128)} %constant.53.clone) | copy-start | bytes 100
  79.6 24.5 %copy-start.14 = (s32[8]{0:T(128)S(1)}, s32[8]{0:T(128)}, u32[]{:S(2)}) copy-start(s32[8]{0:T(128)} %constant.54.clone) | copy-start | bytes 100
  79.6 24.5 %copy-start.15 = (s32[8]{0:T(128)S(1)}, s32[8]{0:T(128)}, u32[]{:S(2)}) copy-start(s32[8]{0:T(128)} %constant.55.clone) | copy-start | bytes 100
  79.7 26.4 %copy-start.1 = (f32[3072]{0:T(1024)S(1)}, f32[3072]{0:T(1024)}, u32[]{:S(2)}) copy-start(f32[3072]{0:T(1024)} %param.31) | copy-start | bytes 36868
  79.7 15.6 %collective-permute-start.12 = (bf16[768,384]{1,0:T(8,128)(2,1)S(1)}, bf16[768,384]{1,0:T(8,128)(2,1)S(1)}, u32[]{:S(2)}, u32[]{:S(2)}) collective-permute-start(bf16[768,384]{1,0:T(8,128)(2,1)S(1)} %fusion.1.refs_0_), channel_id=1, source_target_pairs={{0,2},{2,4},{4,6},{6,0},{1,3},{3,5},{5,7},{7,1},{8,10},{10,12},{12... | collective-permute-start | bytes 1769480 | tf_op jit(solution)/shard_map/ppermute | solution.py:376
  79.7 15.7 %collective-permute-start.13 = (bf16[768,384]{1,0:T(8,128)(2,1)S(1)}, bf16[768,384]{1,0:T(8,128)(2,1)S(1)}, u32[]{:S(2)}, u32[]{:S(2)}) collective-permute-start(bf16[768,384]{1,0:T(8,128)(2,1)S(1)} %fusion.1.refs_0_), channel_id=1, source_target_pairs={{0,6},{2,0},{4,2},{6,4},{1,7},{3,1},{5,3},{7,5},{8,14},{10,8},{12,... | collective-permute-start | bytes 1769480 | tf_op jit(solution)/shard_map/ppermute | solution.py:376
  95.3 8.5 %collective-permute-start.14 = (bf16[384,384]{1,0:T(8,128)(2,1)S(1)}, bf16[384,384]{1,0:T(8,128)(2,1)S(1)}, u32[]{:S(2)}, u32[]{:S(2)}) collective-permute-start(bf16[384,384]{1,0:T(8,128)(2,1)S(1)} %slice.157), channel_id=1, source_target_pairs={{0,2},{2,4},{4,6},{6,0},{1,3},{3,5},{5,7},{7,1},{8,10},{10,12},{12... | collective-permute-start | bytes 884744 | tf_op jit(solution)/shard_map/ppermute | solution.py:376
  95.4 8.4 %collective-permute-start.15 = (bf16[384,384]{1,0:T(8,128)(2,1)S(1)}, bf16[384,384]{1,0:T(8,128)(2,1)S(1)}, u32[]{:S(2)}, u32[]{:S(2)}) collective-permute-start(bf16[384,384]{1,0:T(8,128)(2,1)S(1)} %slice.158), channel_id=1, source_target_pairs={{0,6},{2,0},{4,2},{6,4},{1,7},{3,1},{5,3},{7,5},{8,14},{10,8},{12,... | collective-permute-start | bytes 884744 | tf_op jit(solution)/shard_map/ppermute | solution.py:376
  98.7 6.0 %collective-permute-start.16 = (bf16[768,384]{1,0:T(8,128)(2,1)S(1)}, bf16[768,384]{1,0:T(8,128)(2,1)S(1)}, u32[]{:S(2)}, u32[]{:S(2)}) collective-permute-start(bf16[768,384]{1,0:T(8,128)(2,1)S(1)} %fusion.1.refs_0_), channel_id=1, source_target_pairs={{0,1},{1,0},{2,3},{3,2},{4,5},{5,4},{6,7},{7,6},{8,9},{9,8},{10,11... | collective-permute-start | bytes 1769480 | tf_op jit(solution)/shard_map/ppermute | solution.py:380
  98.7 6.0 %collective-permute-start.17 = (bf16[768,384]{1,0:T(8,128)(2,1)S(1)}, bf16[768,384]{1,0:T(8,128)(2,1)S(1)}, u32[]{:S(2)}, u32[]{:S(2)}) collective-permute-start(bf16[768,384]{1,0:T(8,128)(2,1)S(1)} %collective-permute-done.12.refs_1_), channel_id=1, source_target_pairs={{0,1},{1,0},{2,3},{3,2},{4,5},{5,4},{6,7},{7,6},{8,9},{9,8},{10,11... | collective-permute-start | bytes 1769480 | tf_op jit(solution)/shard_map/ppermute | solution.py:380
  99.2 5.5 %collective-permute-start.18 = (bf16[768,384]{1,0:T(8,128)(2,1)S(1)}, bf16[768,384]{1,0:T(8,128)(2,1)S(1)}, u32[]{:S(2)}, u32[]{:S(2)}) collective-permute-start(bf16[768,384]{1,0:T(8,128)(2,1)S(1)} %collective-permute-done.13.refs_2_), channel_id=1, source_target_pairs={{0,1},{1,0},{2,3},{3,2},{4,5},{5,4},{6,7},{7,6},{8,9},{9,8},{10,11... | collective-permute-start | bytes 1769480 | tf_op jit(solution)/shard_map/ppermute | solution.py:380
  104.0 2.1 collective-permute-start.19
  106.0 7.8 %slice-start = ((f32[3,1056]{1,0:T(4,128)}), f32[3,1024]{1,0:T(4,128)S(1)}, s32[]{:S(2)}) async-start(f32[3,1056]{1,0:T(4,128)} %param.34), calls=%async_computation.1 | async-start | bytes 32768 | tf_op jit(solution)/shard_map/slice | solution.py:448
  111.4 7.5 %collective-permute-start.20 = (bf16[16,3072]{1,0:T(8,128)(2,1)S(1)}, bf16[16,3072]{1,0:T(8,128)(2,1)S(1)}, u32[]{:S(2)}, u32[]{:S(2)}) collective-permute-start(bf16[16,3072]{1,0:T(8,128)(2,1)S(1)} %get-tuple-element.27), channel_id=1, source_target_pairs={{0,8},{8,16},{16,24},{24,32},{32,40},{40,48},{48,56},{56,64},{64,7... | collective-permute-start | bytes 294920 | tf_op jit(solution)/shard_map/ppermute | solution.py:538
  165.7 4.0 %collective-permute-start.22 = (bf16[3,768,384]{2,1,0:T(8,128)(2,1)}, bf16[3,768,384]{2,1,0:T(8,128)(2,1)S(1)}, u32[]{:S(2)}, u32[]{:S(2)}) collective-permute-start(bf16[3,768,384]{2,1,0:T(8,128)(2,1)} %get-tuple-element.33), channel_id=1, source_target_pairs={{0,1},{1,0},{2,3},{3,2},{4,5},{5,4},{6,7},{7,6},{8,9},{9,8},{10,11... | collective-permute-start | bytes 5308424 | tf_op jit(solution)/shard_map/ppermute | solution.py:380
  169.6 4.5 %copy-start = (bf16[768,1152]{1,0:T(8,128)(2,1)S(1)}, bf16[768,1152]{1,0:T(8,128)(2,1)}, u32[]{:S(2)}) copy-start(bf16[768,1152]{1,0:T(8,128)(2,1)} %get-tuple-element.30.h_ref) | copy-start | bytes 5308420
  169.6 4.5 %copy-start.2 = (s32[8]{0:T(128)S(1)}, s32[8]{0:T(128)}, u32[]{:S(2)}) copy-start(s32[8]{0:T(128)} %fusion.13.order_ref) | copy-start | bytes 100
  171.1 14.0 %collective-permute-start.27 = (bf16[384,384]{1,0:T(8,128)(2,1)S(1)}, bf16[384,384]{1,0:T(8,128)(2,1)S(1)}, u32[]{:S(2)}, u32[]{:S(2)}) collective-permute-start(bf16[384,384]{1,0:T(8,128)(2,1)S(1)} %get-tuple-element.45), channel_id=1, source_target_pairs={{0,6},{2,0},{4,2},{6,4},{1,7},{3,1},{5,3},{7,5},{8,14},{10,8},{12,... | collective-permute-start | bytes 884744 | tf_op jit(solution)/shard_map/ppermute | solution.py:376
  177.8 10.9 %collective-permute-start.21 = (bf16[768,384]{1,0:T(8,128)(2,1)S(1)}, bf16[768,384]{1,0:T(8,128)(2,1)S(1)}, u32[]{:S(2)}, u32[]{:S(2)}) collective-permute-start(bf16[768,384]{1,0:T(8,128)(2,1)S(1)} %get-tuple-element.32), channel_id=1, source_target_pairs={{0,1},{1,0},{2,3},{3,2},{4,5},{5,4},{6,7},{7,6},{8,9},{9,8},{10,11... | collective-permute-start | bytes 1769480 | tf_op jit(solution)/shard_map/ppermute | solution.py:380
  177.9 10.6 %collective-permute-start.23 = (bf16[384,384]{1,0:T(8,128)(2,1)S(1)}, bf16[384,384]{1,0:T(8,128)(2,1)S(1)}, u32[]{:S(2)}, u32[]{:S(2)}) collective-permute-start(bf16[384,384]{1,0:T(8,128)(2,1)S(1)} %get-tuple-element.44), channel_id=1, source_target_pairs={{0,2},{2,4},{4,6},{6,0},{1,3},{3,5},{5,7},{7,1},{8,10},{10,12},{12... | collective-permute-start | bytes 884744 | tf_op jit(solution)/shard_map/ppermute | solution.py:376
  181.6 10.7 %collective-permute-start.25 = (bf16[384,384]{1,0:T(8,128)(2,1)S(1)}, bf16[384,384]{1,0:T(8,128)(2,1)S(1)}, u32[]{:S(2)}, u32[]{:S(2)}) collective-permute-start(bf16[384,384]{1,0:T(8,128)(2,1)S(1)} %slice.140), channel_id=1, source_target_pairs={{0,6},{2,0},{4,2},{6,4},{1,7},{3,1},{5,3},{7,5},{8,14},{10,8},{12,... | collective-permute-start | bytes 884744 | tf_op jit(solution)/shard_map/ppermute | solution.py:376
  185.0 11.2 %collective-permute-start.26 = (bf16[384,384]{1,0:T(8,128)(2,1)S(1)}, bf16[384,384]{1,0:T(8,128)(2,1)S(1)}, u32[]{:S(2)}, u32[]{:S(2)}) collective-permute-start(bf16[384,384]{1,0:T(8,128)(2,1)S(1)} %slice.142), channel_id=1, source_target_pairs={{0,2},{2,4},{4,6},{6,0},{1,3},{3,5},{5,7},{7,1},{8,10},{10,12},{12... | collective-permute-start | bytes 884744 | tf_op jit(solution)/shard_map/ppermute | solution.py:376
  185.1 12.7 %collective-permute-start.28 = (bf16[384,384]{1,0:T(8,128)(2,1)S(1)}, bf16[384,384]{1,0:T(8,128)(2,1)S(1)}, u32[]{:S(2)}, u32[]{:S(2)}) collective-permute-start(bf16[384,384]{1,0:T(8,128)(2,1)S(1)} %add_convert_fusion.4), channel_id=1, source_target_pairs={{0,6},{2,0},{4,2},{6,4},{1,7},{3,1},{5,3},{7,5},{8,14},{10,8},{12,... | collective-permute-start | bytes 884744 | tf_op jit(solution)/shard_map/ppermute | solution.py:376
  188.6 12.8 %collective-permute-start.24 = (bf16[384,384]{1,0:T(8,128)(2,1)S(1)}, bf16[384,384]{1,0:T(8,128)(2,1)S(1)}, u32[]{:S(2)}, u32[]{:S(2)}) collective-permute-start(bf16[384,384]{1,0:T(8,128)(2,1)S(1)} %add_convert_fusion.5), channel_id=1, source_target_pairs={{0,2},{2,4},{4,6},{6,0},{1,3},{3,5},{5,7},{7,1},{8,10},{10,12},{12... | collective-permute-start | bytes 884744 | tf_op jit(solution)/shard_map/ppermute | solution.py:376
  (4 other events, 2.5 us)
Sparse Core Ops, SparseCore 0:
  9.5 132.0 all-gather.1
where the time goes:
time: 210 us; the launch traced here: 209 us
  waiting for transfers between devices  78.3 us (37%)
  Pallas kernels  54.4 us (26%)
  starting transfers between devices  47.3 us (23%)
  between operations  13.9 us (7%)
  local copies, waits for them, and re-layouts  9.95 us (5%)
  other arithmetic  5.5 us (3%)
    ppermute x16, waiting for transfers between devices, shifted(): return lax.ppermute(value, 'y', [(i, (i + by) % ring) for i in range(ring)])  44.6 us
    ppermute x16, starting transfers between devices, shifted(): return lax.ppermute(value, 'y', [(i, (i + by) % ring) for i in range(ring)])  26.7 us
    pallas_call x1, Pallas kernels, layer(): pl.pallas_call(mixer_kernel, grid_spec=pltpu.PrefetchScalarGridSpec(num_s...  24.1 us
    all_gather x1, waiting for transfers between devices, layer(): weights = lax.all_gather(packed, SP, axis=0, tiled=True)  22.1 us
    ppermute x4, starting transfers between devices, layer(): lax.ppermute(pay, SP, [(i, i + k) for i in range(count - k)])  16.7 us
    pallas_call x1, Pallas kernels, layer(): pl.pallas_call(mix_kernel, grid_spec=pltpu.PrefetchScalarGridSpec(num_sca...  7.97 us
    pallas_call x2, Pallas kernels, more(): pl.pallas_call(kernel, grid_spec=pltpu.PrefetchScalarGridSpec(num_scalar_...  7.32 us
    ppermute x8, waiting for transfers between devices, swapped(): return lax.ppermute(value, 'c', [(0, 1), (1, 0)])  7.2 us
  transfers between devices with their start and end apart: 30, of which 16 were waited for; matrix products, arithmetic and copies ran while one was open for 5% of the time, Pallas kernels for 13%

commit v1 on v0

--- a/solution.py
+++ b/solution.py
@@ -23,15 +23,32 @@
     return lax.broadcasted_iota(jnp.int32, shape, len(shape) - 1) < DH
 
 
-def pack_kernel(gate_ref, value_ref, down_ref, out_ref):
+def pack_kernel(gate_ref, value_ref, down_ref, out_ref, tails, last, sems):
     rows, hidden = gate_ref.shape
-    main = hidden // 128 * 128
-    tails = []
+    spare = tails.shape[2]
+    main = hidden - spare
+    ends, mains = [], []
     for k, ref in enumerate((gate_ref, value_ref, down_ref)):
-        out_ref[:, k * main : (k + 1) * main] = ref[:, :main]
-        tails.append(ref[:, main:])
-    tails.append(jnp.zeros((rows, 128 - 3 * (hidden - main)), BF16))
-    out_ref[:, 3 * main :] = jnp.concatenate(tails, axis=1)
+        ends.append(
+            pltpu.make_async_copy(ref.at[:, pl.ds(main, spare)], tails.at[k], sems.at[k])
+        )
+        mains.append(
+            pltpu.make_async_copy(
+                ref.at[:, pl.ds(0, main)], out_ref.at[:, pl.ds(k * main, main)], sems.at[3 + k]
+            )
+        )
+    for copy in ends + mains:
+        copy.start()
+    for copy in ends:
+        copy.wait()
+    last[...] = jnp.concatenate(
+        [tails[0], tails[1], tails[2], jnp.zeros((rows, 128 - 3 * spare), BF16)], axis=1
+    )
+    end = pltpu.make_async_copy(last, out_ref.at[:, pl.ds(3 * main, 128)], sems.at[6])
+    end.start()
+    for copy in mains:
+        copy.wait()
+    end.wait()
 
 
 def state_kernel(k_ref, v_ref, in_ref, forget_ref, doc_ref, pay_ref, row_ref, col_ref, scr):
@@ -210,14 +227,16 @@
     taps_ref,
     wg_ref,
     wv_ref,
-    wt_ref,
     w_ref,
     h_ref,
+    far_swap_ref,
     swap_ref,
     own_ref,
     gate_scr,
     value_scr,
     tail_scr,
+    x_scr,
+    wt_scr,
     down_scr,
     sems,
 ):
@@ -244,6 +263,14 @@
             ),
         )
 
+    depth = x_scr.shape[1] // 4
+    x_cuts = [pl.ds(k * depth, depth) for k in range(4)]
+    x_copies = [
+        pltpu.make_async_copy(x_ref.at[:, cut], x_scr.at[:, cut], sems.at[8 + k])
+        for k, cut in enumerate(x_cuts)
+    ]
+    wt_copy = pltpu.make_async_copy(w_ref.at[:, pl.ds(3 * main, 128)], wt_scr, sems.at[12])
+
     def hidden(gate, value, taps, rows):
         near, far = near_ref[rows, :], far_ref[rows, :]
         one = pltpu.roll(gate, 1, 0)[HALO:, :]
@@ -287,8 +314,8 @@
             h_ref[start : start + block, main:] = jnp.where(mine, done, 0.0).astype(BF16)
 
     def project(slot):
-        gate_scr[slot] = jnp.dot(x_ref[...], wg_ref[...], preferred_element_type=F32)
-        value_scr[slot] = jnp.dot(x_ref[...], wv_ref[...], preferred_element_type=F32)
+        gate_scr[slot] = jnp.dot(x_scr[...], wg_ref[...], preferred_element_type=F32)
+        value_scr[slot] = jnp.dot(x_scr[...], wv_ref[...], preferred_element_type=F32)
 
     def product(n, cuts):
         total = None
@@ -304,14 +331,26 @@
 
     @pl.when(j == 0)
     def _():
+        for copy in (*x_copies, wt_copy):
+            copy.start()
         for n in range(2 * pairs):
             for copy in copies(n):
                 copy.start()
-        tail_scr[...] = jnp.dot(x_ref[...], wt_ref[...], preferred_element_type=F32)
-        project(0)
+        gate = value = None
+        for cut, copy in zip(x_cuts, x_copies):
+            copy.wait()
+            x = x_scr[:, cut]
+            gate_part = jnp.dot(x, wg_ref[cut, :], preferred_element_type=F32)
+            value_part = jnp.dot(x, wv_ref[cut, :], preferred_element_type=F32)
+            gate = gate_part if gate is None else gate + gate_part
+            value = value_part if value is None else value + value_part
+        gate_scr[0] = gate
+        value_scr[0] = value
 
     @pl.when(j == 1)
     def _():
+        wt_copy.wait()
+        tail_scr[...] = jnp.dot(x_scr[...], wt_scr[...], preferred_element_type=F32)
         project(1)
         finish_tail()
         finish(0, 0)
@@ -329,7 +368,7 @@
                 copy.wait()
         known = main - tile
         both = product(0, (slice(0, known), slice(main, main + 128), slice(known, main)))
-        swap_ref[0], own_ref[0] = both[:, :cols], both[:, cols:]
+        far_swap_ref[0], own_ref[0] = both[:, :cols], both[:, cols:]
 
     @pl.when(j > tiles)
     def _():
@@ -337,7 +376,7 @@
             for copy in copies(n):
                 copy.wait()
         both = product(1, (slice(None),))
-        swap_ref[1], swap_ref[2] = both[:, :cols], both[:, cols:]
+        swap_ref[0], swap_ref[1] = both[:, :cols], both[:, cols:]
 
 
 def two_parts(h_ref, wa_ref, wb_ref, ta_ref, tb_ref):
@@ -380,9 +419,10 @@
     return lax.ppermute(value, "c", [(0, 1), (1, 0)])
 
 
-def summed_over_tp(swap, own, sides, last):
+def summed_over_tp(far_swap, swap, own, sides, last):
+    far_swap = swapped(far_swap)
     other = swapped(swap)
-    far = added(own, other[0]).astype(BF16)
+    far = added(own, far_swap).astype(BF16)
     half = far.shape[0] // 2
     far_up, far_down = shifted(far[:half], 1), shifted(far[half:], -1)
     up, down = sides(other)
@@ -436,7 +476,14 @@
     spare = hidden - main
     packed = pl.pallas_call(
         pack_kernel,
+        in_specs=[pl.BlockSpec(memory_space=pl.ANY)] * 3,
+        out_specs=pl.BlockSpec(memory_space=pl.ANY),
         out_shape=shape((w_gate.shape[0], 3 * main + 128), BF16),
+        scratch_shapes=[
+            pltpu.VMEM((3, w_gate.shape[0], spare), BF16),
+            pltpu.VMEM((w_gate.shape[0], 128), BF16),
+            pltpu.SemaphoreType.DMA((7,)),
+        ],
         name="pack",
     )(w_gate, w_value, w_down.T)
     weights = lax.all_gather(packed, SP, axis=0, tiled=True)
@@ -509,9 +556,10 @@
         name="mix",
     )(order, query, out_gate, local, rows, cols_aux, head_gain.reshape(1, width), w_out, w_out, *pays)
     attended = summed_over_tp(
-        swap[:3],
+        swap[0],
+        swap[1:3],
         own[0],
-        lambda other: tuple(added(own[k], other[k]).astype(BF16) for k in (1, 2)),
+        lambda other: tuple(added(own[1 + k], other[k]).astype(BF16) for k in range(2)),
         lambda: (swap[3], own[3]),
     )
     residual_own = resid.astype(F32) + jnp.concatenate(attended, axis=0)
@@ -541,15 +589,13 @@
     order = (chip + jnp.array([2, 2, 1, 3, 1, 3, 0, 0], jnp.int32)) % ring * cores + (
         core ^ jnp.array([1, 0, 1, 1, 0, 0, 1, 0], jnp.int32)
     )
-    hidden, swap, own = pl.pallas_call(
+    hidden, far_swap, swap, own = pl.pallas_call(
         mixer_kernel,
         grid_spec=pltpu.PrefetchScalarGridSpec(
             num_scalar_prefetch=1,
             grid=(tiles + 2,),
             in_specs=[
-                pl.BlockSpec(
-                    (tokens + HALO, model), lambda j, order: (0, 0), pipeline_mode=pl.Buffered(1)
-                ),
+                pl.BlockSpec(memory_space=pl.ANY),
                 whole((tokens, 128)),
                 whole((tokens, 128)),
                 whole((tiles + 1, 3, tile)),
@@ -557,32 +603,33 @@
                 pl.BlockSpec(
                     (model, tile), lambda j, order: (0, tiles + jnp.minimum(j, tiles - 1))
                 ),
-                pl.BlockSpec(
-                    (model, 128), lambda j, order: (0, tail_at), pipeline_mode=pl.Buffered(1)
-                ),
                 pl.BlockSpec(memory_space=pl.ANY),
             ],
             out_specs=(
                 whole((tokens, main + 128)),
-                whole((3, tokens, cols)),
+                whole((1, tokens, cols)),
+                whole((2, tokens, cols)),
                 whole((1, tokens, cols)),
             ),
             scratch_shapes=[
                 pltpu.VMEM((2, tokens + HALO, tile), F32),
                 pltpu.VMEM((2, tokens + HALO, tile), F32),
                 pltpu.VMEM((tokens + HALO, 128), F32),
+                pltpu.VMEM((tokens + HALO, model), BF16),
+                pltpu.VMEM((model, 128), BF16),
                 pltpu.VMEM((2, 2 * cols, main + 128), BF16),
-                pltpu.SemaphoreType.DMA((8,)),
+                pltpu.SemaphoreType.DMA((13,)),
             ],
         ),
         out_shape=(
             shape((tokens, main + 128), BF16),
-            shape((3, tokens, cols), BF16),
+            shape((1, tokens, cols), BF16),
+            shape((2, tokens, cols), BF16),
             shape((1, tokens, cols), BF16),
         ),
         compiler_params=pltpu.CompilerParams(vmem_limit_bytes=58 * 2**20),
         name="mixer",
-    )(order, normed, near, far_flags, taps, *[weights] * 4)
+    )(order, normed, near, far_flags, taps, *[weights] * 3)
 
     def more(kernel, at, given, specs):
         def spot(k, col):
@@ -609,13 +656,14 @@
         )(order, hidden, *[weights] * 4, *given)
 
     down = summed_over_tp(
+        far_swap[0],
         swap,
         own[0],
         lambda other: more(
             side_kernel,
             4,
             (other, other),
-            [pl.BlockSpec((1, tokens, cols), lambda j, order, k=k: (k, 0, 0)) for k in (1, 2)],
+            [pl.BlockSpec((1, tokens, cols), lambda j, order, k=k: (k, 0, 0)) for k in (0, 1)],
         ),
         lambda: more(down_kernel, 6, (), []),
     )

time: 210 us -> 246 us (1.17)
  Pallas kernels: 54.4 us -> 89.2 us
    pallas_call x1, Pallas kernels: 2.5 us -> 36.9 us  [layer(): pl.pallas_call(pack_kernel, in_specs=[pl.BlockSpec(memory_space=pl.ANY)]...]
    ppermute x16, waiting for transfers between devices: 44.6 us -> 50.2 us  [shifted(): return lax.ppermute(value, 'y', [(i, (i + by) % ring) for i in range(ring)])]
    all_gather x1, waiting for transfers between devices: 22.1 us -> 18.2 us  [layer(): weights = lax.all_gather(packed, SP, axis=0, tiled=True)]
    unnamed x45 -> x47, local copies, waits for them, and re-layouts: 5.35 us -> 6.63 us
    ppermute x8 -> x10, waiting for transfers between devices: 7.2 us -> 6.47 us  [swapped(): return lax.ppermute(value, 'c', [(0, 1), (1, 0)])]
  transfers between devices with their start and end apart: 30 -> 32, of which waited for: 16 -> 15; matrix products, arithmetic and copies ran while one was open for 5% -> 5% of each run, Pallas kernels for 13% -> 11%
where the time goes in v1:
time: 246 us; the launch traced here: 245 us
  Pallas kernels  89.2 us (36%)
  waiting for transfers between devices  79.2 us (32%)
  starting transfers between devices  47.7 us (19%)
  between operations  13.9 us (6%)
  local copies, waits for them, and re-layouts  9.96 us (4%)
  other arithmetic  5.52 us (2%)
    ppermute x16, waiting for transfers between devices, shifted(): return lax.ppermute(value, 'y', [(i, (i + by) % ring) for i in range(ring)])  50.2 us
    pallas_call x1, Pallas kernels, layer(): pl.pallas_call(pack_kernel, in_specs=[pl.BlockSpec(memory_space=pl.ANY)]...  36.9 us
    ppermute x16, starting transfers between devices, shifted(): return lax.ppermute(value, 'y', [(i, (i + by) % ring) for i in range(ring)])  26.5 us
    pallas_call x1, Pallas kernels, layer(): pl.pallas_call(mixer_kernel, grid_spec=pltpu.PrefetchScalarGridSpec(num_s...  24.4 us
    all_gather x1, waiting for transfers between devices, layer(): weights = lax.all_gather(packed, SP, axis=0, tiled=True)  18.2 us
    ppermute x4, starting transfers between devices, layer(): lax.ppermute(pay, SP, [(i, i + k) for i in range(count - k)])  16.7 us
    pallas_call x1, Pallas kernels, layer(): pl.pallas_call(mix_kernel, grid_spec=pltpu.PrefetchScalarGridSpec(num_sca...  7.95 us
    pallas_call x2, Pallas kernels, more(): pl.pallas_call(kernel, grid_spec=pltpu.PrefetchScalarGridSpec(num_scalar_...  7.31 us
  transfers between devices with their start and end apart: 32, of which 15 were waited for; matrix products, arithmetic and copies ran while one was open for 5% of the time, Pallas kernels for 11%

profile of v1, /device:TPU:0, one launch (start us, length us, event | category | flops | bytes accessed | tf_op | source)
XLA Modules:
  0.0 245.5 jit_solution(8558905081815076570)
XLA Ops:
  6.5 36.9 %pack.1 = bf16[192,3200]{1,0:T(8,128)(2,1)} custom-call(bf16[192,1056]{1,0:T(8,128)(2,1)} %gate_ref.2, bf16[192,1056]{1,0:T(8,128)(2,1)} %value_ref.1, bf16[192,1056]{1,0:T(8,128)(2,1)} %bitcast.37), custom_call_target="tpu_custom_call" | custom-call | tf_op jit(solution)/shard_map/pack/pallas_call | solution.py:477
  43.5 0.9 copy-done.6
  44.4 0.9 copy.25.k_ref
  45.3 0.9 copy.26.v_ref
  46.3 0.6 reshape.34.doc_ref
  46.8 3.6 %state.1 = (bf16[112,192]{1,0:T(8,128)(2,1)}, f32[8,768]{1,0:T(8,128)}, f32[768,8]{1,0:T(8,128)}) custom-call(bf16[768,192]{1,0:T(8,128)(2,1)} %copy.25.k_ref, bf16[768,192]{1,0:T(8,128)(2,1)} %copy.26.v_ref, f32[2,768]{1,0:T(2,128)} %in_ref.1, f32[2,768]{1,0:T(2,128)} %forget_ref.1, s32[1,768]{1,0:T(1,128)} %reshape.34.doc_ref), custom_call_target="tpu_custom_call" | custom-call | tf_op jit(solution)/shard_map/state/pallas_call | solution.py:501
  50.5 3.5 %collective-permute-start = (bf16[112,192]{1,0:T(8,128)(2,1)}, bf16[112,192]{1,0:T(8,128)(2,1)S(1)}, u32[]{:S(2)}, u32[]{:S(2)}) collective-permute-start(bf16[112,192]{1,0:T(8,128)(2,1)} %get-tuple-element.24), channel_id=1, source_target_pairs={{0,8},{8,16},{16,24},{24,32},{32,40},{40,48},{48,56},{56,64},{64,7... | collective-permute-start | bytes 129032 | tf_op jit(solution)/shard_map/ppermute | solution.py:514
  54.0 4.6 %collective-permute-start.1 = (bf16[112,192]{1,0:T(8,128)(2,1)}, bf16[112,192]{1,0:T(8,128)(2,1)S(1)}, u32[]{:S(2)}, u32[]{:S(2)}) collective-permute-start(bf16[112,192]{1,0:T(8,128)(2,1)} %get-tuple-element.24), channel_id=1, source_target_pairs={{0,16},{8,24},{16,32},{24,40},{32,48},{40,56},{48,64},{56,72},{64,... | collective-permute-start | bytes 129032 | tf_op jit(solution)/shard_map/ppermute | solution.py:514
  58.6 4.7 %collective-permute-start.2 = (bf16[112,192]{1,0:T(8,128)(2,1)}, bf16[112,192]{1,0:T(8,128)(2,1)S(1)}, u32[]{:S(2)}, u32[]{:S(2)}) collective-permute-start(bf16[112,192]{1,0:T(8,128)(2,1)} %get-tuple-element.24), channel_id=1, source_target_pairs={{0,24},{8,32},{16,40},{24,48},{32,56},{40,64},{48,72},{56,80},{64,... | collective-permute-start | bytes 129032 | tf_op jit(solution)/shard_map/ppermute | solution.py:514
  63.3 3.8 %collective-permute-start.3 = (bf16[112,192]{1,0:T(8,128)(2,1)}, bf16[112,192]{1,0:T(8,128)(2,1)S(1)}, u32[]{:S(2)}, u32[]{:S(2)}) collective-permute-start(bf16[112,192]{1,0:T(8,128)(2,1)} %get-tuple-element.24), channel_id=1, source_target_pairs={{0,32},{8,40},{16,48},{24,56},{32,64},{40,72},{48,80},{56,88},{64,... | collective-permute-start | bytes 129032 | tf_op jit(solution)/shard_map/ppermute | solution.py:514
  67.7 0.9 copy.27.q_ref
  68.6 0.9 copy.28.gate_ref
  69.6 3.7 %local.1.local_ref = f32[768,192]{1,0:T(8,128)} custom-call(bf16[768,192]{1,0:T(8,128)(2,1)} %copy.27.q_ref, bf16[768,192]{1,0:T(8,128)(2,1)} %copy.25.k_ref, bf16[768,192]{1,0:T(8,128)(2,1)} %copy.26.v_ref, f32[8,768]{1,0:T(8,128)} %get-tuple-element.22.row_ref, f32[768,8]{1,0:T(8,128)} %get-tuple-element.23.col_ref), custom_call_target="tpu_custom_call" | custom-call | tf_op jit(solution)/shard_map/local/pallas_call | solution.py:516
  73.9 7.9 %mix.1 = (bf16[4,768,384]{2,1,0:T(8,128)(2,1)}, bf16[4,768,384]{2,1,0:T(8,128)(2,1)}, f32[768,128]{1,0:T(8,128)}, f32[768,128]{1,0:T(8,128)}) custom-call(s32[8]{0:T(128)} %fusion.12.order_ref, bf16[768,192]{1,0:T(8,128)(2,1)} %copy.27.q_ref, bf16[768,192]{1,0:T(8,128)(2,1)} %copy.28.gate_ref, f32[768,192]{1,0:T(8,128)} %local.1.local_ref, ...), custom_call_target="tpu_custom_call" | custom-call | tf_op jit(solution)/shard_map/mix/pallas_call | solution.py:526
  81.9 1.5 slice.99
  84.6 2.6 %collective-permute-done.4 = bf16[768,384]{1,0:T(8,128)(2,1)S(1)} collective-permute-done((bf16[768,384]{1,0:T(8,128)(2,1)S(1)}, bf16[768,384]{1,0:T(8,128)(2,1)S(1)}, u32[]{:S(2)}, u32[]{:S(2)}) %collective-permute-start.4) | collective-permute-done | bytes 589856 | tf_op jit(solution)/shard_map/ppermute | solution.py:419
  87.2 0.8 collective-permute-done.6
  88.4 3.0 %collective-permute-start.11 = (bf16[384,384]{1,0:T(8,128)(2,1)S(1)}, bf16[384,384]{1,0:T(8,128)(2,1)S(1)}, u32[]{:S(2)}, u32[]{:S(2)}) collective-permute-start(bf16[384,384]{1,0:T(8,128)(2,1)S(1)} %get-tuple-element.52), channel_id=1, source_target_pairs={{0,6},{2,0},{4,2},{6,4},{1,7},{3,1},{5,3},{7,5},{8,14},{10,8},{12,... | collective-permute-start | bytes 884744 | tf_op jit(solution)/shard_map/ppermute | solution.py:415
  91.8 6.2 %collective-permute-done.11 = bf16[384,384]{1,0:T(8,128)(2,1)S(1)} collective-permute-done((bf16[384,384]{1,0:T(8,128)(2,1)S(1)}, bf16[384,384]{1,0:T(8,128)(2,1)S(1)}, u32[]{:S(2)}, u32[]{:S(2)}) %collective-permute-start.11) | collective-permute-done | bytes 294944 | tf_op jit(solution)/shard_map/ppermute | solution.py:415
  98.1 3.8 %collective-permute-start.12 = (bf16[384,384]{1,0:T(8,128)(2,1)S(1)}, bf16[384,384]{1,0:T(8,128)(2,1)S(1)}, u32[]{:S(2)}, u32[]{:S(2)}) collective-permute-start(bf16[384,384]{1,0:T(8,128)(2,1)S(1)} %fusion.8), channel_id=1, source_target_pairs={{0,6},{2,0},{4,2},{6,4},{1,7},{3,1},{5,3},{7,5},{8,14},{10,8},{12,... | collective-permute-start | bytes 884744 | tf_op jit(solution)/shard_map/ppermute | solution.py:415
  102.2 3.2 %collective-permute-start.9 = (bf16[384,384]{1,0:T(8,128)(2,1)S(1)}, bf16[384,384]{1,0:T(8,128)(2,1)S(1)}, u32[]{:S(2)}, u32[]{:S(2)}) collective-permute-start(bf16[384,384]{1,0:T(8,128)(2,1)S(1)} %slice_bitcast_fusion.4), channel_id=1, source_target_pairs={{0,6},{2,0},{4,2},{6,4},{1,7},{3,1},{5,3},{7,5},{8,14},{10,8},{12,... | collective-permute-start | bytes 884744 | tf_op jit(solution)/shard_map/ppermute | solution.py:415
  105.4 3.9 %collective-permute-done.12 = bf16[384,384]{1,0:T(8,128)(2,1)S(1)} collective-permute-done((bf16[384,384]{1,0:T(8,128)(2,1)S(1)}, bf16[384,384]{1,0:T(8,128)(2,1)S(1)}, u32[]{:S(2)}, u32[]{:S(2)}) %collective-permute-start.12) | collective-permute-done | bytes 294944 | tf_op jit(solution)/shard_map/ppermute | solution.py:415
  109.3 3.9 %collective-permute-done.8 = bf16[384,384]{1,0:T(8,128)(2,1)S(1)} collective-permute-done((bf16[384,384]{1,0:T(8,128)(2,1)S(1)}, bf16[384,384]{1,0:T(8,128)(2,1)S(1)}, u32[]{:S(2)}, u32[]{:S(2)}) %collective-permute-start.8) | collective-permute-done | bytes 294944 | tf_op jit(solution)/shard_map/ppermute | solution.py:415
  113.2 4.5 %collective-permute-done.10 = bf16[384,384]{1,0:T(8,128)(2,1)S(1)} collective-permute-done((bf16[384,384]{1,0:T(8,128)(2,1)S(1)}, bf16[384,384]{1,0:T(8,128)(2,1)S(1)}, u32[]{:S(2)}, u32[]{:S(2)}) %collective-permute-start.10) | collective-permute-done | bytes 294944 | tf_op jit(solution)/shard_map/ppermute | solution.py:415
  117.8 0.9 copy-done.5
  119.0 3.2 %collective-permute-start.14 = (bf16[768,384]{1,0:T(8,128)(2,1)S(1)}, bf16[768,384]{1,0:T(8,128)(2,1)S(1)}, u32[]{:S(2)}, u32[]{:S(2)}) collective-permute-start(bf16[768,384]{1,0:T(8,128)(2,1)S(1)} %fusion.3.refs_0_), channel_id=1, source_target_pairs={{0,6},{2,0},{4,2},{6,4},{1,7},{3,1},{5,3},{7,5},{8,14},{10,8},{12,... | collective-permute-start | bytes 1769480 | tf_op jit(solution)/shard_map/ppermute | solution.py:415
  122.2 11.6 %collective-permute-done.13.refs_1_ = bf16[768,384]{1,0:T(8,128)(2,1)S(1)} collective-permute-done((bf16[768,384]{1,0:T(8,128)(2,1)S(1)}, bf16[768,384]{1,0:T(8,128)(2,1)S(1)}, u32[]{:S(2)}, u32[]{:S(2)}) %collective-permute-start.13) | collective-permute-done | bytes 589856 | tf_op jit(solution)/shard_map/ppermute | solution.py:415
  133.9 3.3 %collective-permute-start.16 = (bf16[384,384]{1,0:T(8,128)(2,1)S(1)}, bf16[384,384]{1,0:T(8,128)(2,1)S(1)}, u32[]{:S(2)}, u32[]{:S(2)}) collective-permute-start(bf16[384,384]{1,0:T(8,128)(2,1)S(1)} %slice.137), channel_id=1, source_target_pairs={{0,6},{2,0},{4,2},{6,4},{1,7},{3,1},{5,3},{7,5},{8,14},{10,8},{12,... | collective-permute-start | bytes 884744 | tf_op jit(solution)/shard_map/ppermute | solution.py:415
  137.7 4.1 %collective-permute-done.15 = bf16[384,384]{1,0:T(8,128)(2,1)S(1)} collective-permute-done((bf16[384,384]{1,0:T(8,128)(2,1)S(1)}, bf16[384,384]{1,0:T(8,128)(2,1)S(1)}, u32[]{:S(2)}, u32[]{:S(2)}) %collective-permute-start.15) | collective-permute-done | bytes 294944 | tf_op jit(solution)/shard_map/ppermute | solution.py:415
  142.7 1.3 collective-permute-done.20.refs_7_
  144.0 5.3 %norm.1 = (bf16[784,3072]{1,0:T(8,128)(2,1)}, bf16[16,3072]{1,0:T(8,128)(2,1)S(1)}) custom-call(s32[8]{0:T(128)S(1)} %fusion.18.order_ref, bf16[768,384]{1,0:T(8,128)(2,1)S(1)} %fusion.3.refs_0_, bf16[768,384]{1,0:T(8,128)(2,1)S(1)} %collective-permute-done.13.refs_1_, bf16[768,384]{1,0:T(8,128)(2,1)S(1)} %collective-permute-done.14.refs_2_, ...), custom_call_target="tpu_custom_call" | custom-call | tf_op jit(solution)/shard_map/norm/pallas_call | solution.py:571
  149.4 2.6 %collective-permute-start.21 = (bf16[16,3072]{1,0:T(8,128)(2,1)S(1)}, bf16[16,3072]{1,0:T(8,128)(2,1)S(1)}, u32[]{:S(2)}, u32[]{:S(2)}) collective-permute-start(bf16[16,3072]{1,0:T(8,128)(2,1)S(1)} %get-tuple-element.28), channel_id=1, source_target_pairs={{0,8},{8,16},{16,24},{24,32},{32,40},{40,48},{48,56},{56,64},{64,7... | collective-permute-start | bytes 294920 | tf_op jit(solution)/shard_map/ppermute | solution.py:586
  151.9 0.6 pad_maximum_fusion.taps_ref
  152.5 4.4 %collective-permute-done.21 = bf16[16,3072]{1,0:T(8,128)(2,1)S(1)} collective-permute-done((bf16[16,3072]{1,0:T(8,128)(2,1)S(1)}, bf16[16,3072]{1,0:T(8,128)(2,1)S(1)}, u32[]{:S(2)}, u32[]{:S(2)}) %collective-permute-start.21) | collective-permute-done | bytes 98336 | tf_op jit(solution)/shard_map/ppermute | solution.py:586
  157.0 0.6 constant_dynamic-update-slice_fusion.2.x_ref
  157.6 18.2 %all-gather.2.cloned.1.call-done.wg_ref.wv_ref.w_ref.wa_ref.wb_ref.ta_ref.tb_ref = bf16[3072,3200]{1,0:T(8,128)(2,1)} async-done(((bf16[192,3200]{1,0:T(8,128)(2,1)}), bf16[3072,3200]{1,0:T(8,128)(2,1)}) %all-gather.2.cloned.1.call-update) | async-done | bytes 19660816 | tf_op jit(solution)/shard_map/all_gather | solution.py:489
  175.8 24.4 %mixer.1 = (bf16[768,1152]{1,0:T(8,128)(2,1)}, bf16[1,768,384]{2,1,0:T(8,128)(2,1)}, bf16[2,768,384]{2,1,0:T(8,128)(2,1)}, bf16[1,768,384]{2,1,0:T(8,128)(2,1)}) custom-call(s32[8]{0:T(128)} %fusion.15.order_ref, bf16[784,3072]{1,0:T(8,128)(2,1)} %constant_dynamic-update-slice_fusion.2.x_ref, f32[768,128]{1,0:T(8,128)} %get-tuple-element.29.near_ref, ...), custom_call_target="tpu_custom_call" | custom-call | tf_op jit(solution)/shard_map/mixer/pallas_call | solution.py:592
  200.8 1.7 collective-permute-done.24
  202.5 1.3 fusion.1
  203.9 3.0 %collective-permute-start.29 = (bf16[384,384]{1,0:T(8,128)(2,1)S(1)}, bf16[384,384]{1,0:T(8,128)(2,1)S(1)}, u32[]{:S(2)}, u32[]{:S(2)}) collective-permute-start(bf16[384,384]{1,0:T(8,128)(2,1)S(1)} %get-tuple-element.50), channel_id=1, source_target_pairs={{0,6},{2,0},{4,2},{6,4},{1,7},{3,1},{5,3},{7,5},{8,14},{10,8},{12,... | collective-permute-start | bytes 884744 | tf_op jit(solution)/shard_map/ppermute | solution.py:415
  206.9 3.6 %shard_map.199 = (bf16[768,384]{1,0:T(8,128)(2,1)S(1)}, bf16[768,384]{1,0:T(8,128)(2,1)S(1)}) custom-call(s32[8]{0:T(128)S(1)} %copy-done.2, bf16[768,1152]{1,0:T(8,128)(2,1)S(1)} %copy-done, bf16[3072,3200]{1,0:T(8,128)(2,1)} %all-gather.2.cloned.1.call-done.wg_ref.wv_ref.w_ref.wa_ref.wb_ref.ta_ref.tb_ref, ...), custom_call_target="tpu_custom_call" | custom-call | tf_op jit(solution)/shard_map/pallas_call | solution.py:639
  210.8 3.7 %shard_map.200 = (bf16[768,384]{1,0:T(8,128)(2,1)S(1)}, bf16[768,384]{1,0:T(8,128)(2,1)S(1)}) custom-call(s32[8]{0:T(128)S(1)} %copy-done.2, bf16[768,1152]{1,0:T(8,128)(2,1)S(1)} %copy-done, bf16[3072,3200]{1,0:T(8,128)(2,1)} %all-gather.2.cloned.1.call-done.wg_ref.wv_ref.w_ref.wa_ref.wb_ref.ta_ref.tb_ref, ...), custom_call_target="tpu_custom_call" | custom-call | tf_op jit(solution)/shard_map/pallas_call | solution.py:639
  214.6 3.3 %collective-permute-start.30 = (bf16[384,384]{1,0:T(8,128)(2,1)S(1)}, bf16[384,384]{1,0:T(8,128)(2,1)S(1)}, u32[]{:S(2)}, u32[]{:S(2)}) collective-permute-start(bf16[384,384]{1,0:T(8,128)(2,1)S(1)} %add_convert_fusion.2), channel_id=1, source_target_pairs={{0,6},{2,0},{4,2},{6,4},{1,7},{3,1},{5,3},{7,5},{8,14},{10,8},{12,... | collective-permute-start | bytes 884744 | tf_op jit(solution)/shard_map/ppermute | solution.py:415
  217.9 3.4 %collective-permute-done.25 = bf16[384,384]{1,0:T(8,128)(2,1)S(1)} collective-permute-done((bf16[384,384]{1,0:T(8,128)(2,1)S(1)}, bf16[384,384]{1,0:T(8,128)(2,1)S(1)}, u32[]{:S(2)}, u32[]{:S(2)}) %collective-permute-start.25) | collective-permute-done | bytes 294944 | tf_op jit(solution)/shard_map/ppermute | solution.py:415
  221.5 3.2 %collective-permute-start.27 = (bf16[384,384]{1,0:T(8,128)(2,1)S(1)}, bf16[384,384]{1,0:T(8,128)(2,1)S(1)}, u32[]{:S(2)}, u32[]{:S(2)}) collective-permute-start(bf16[384,384]{1,0:T(8,128)(2,1)S(1)} %slice.121), channel_id=1, source_target_pairs={{0,6},{2,0},{4,2},{6,4},{1,7},{3,1},{5,3},{7,5},{8,14},{10,8},{12,... | collective-permute-start | bytes 884744 | tf_op jit(solution)/shard_map/ppermute | solution.py:415
  224.8 7.7 %collective-permute-done.26 = bf16[384,384]{1,0:T(8,128)(2,1)S(1)} collective-permute-done((bf16[384,384]{1,0:T(8,128)(2,1)S(1)}, bf16[384,384]{1,0:T(8,128)(2,1)S(1)}, u32[]{:S(2)}, u32[]{:S(2)}) %collective-permute-start.26) | collective-permute-done | bytes 294944 | tf_op jit(solution)/shard_map/ppermute | solution.py:415
  232.5 4.9 %collective-permute-done.28 = bf16[384,384]{1,0:T(8,128)(2,1)S(1)} collective-permute-done((bf16[384,384]{1,0:T(8,128)(2,1)S(1)}, bf16[384,384]{1,0:T(8,128)(2,1)S(1)}, u32[]{:S(2)}, u32[]{:S(2)}) %collective-permute-start.28) | collective-permute-done | bytes 294944 | tf_op jit(solution)/shard_map/ppermute | solution.py:415
  237.6 1.0 fusion
  (106 shorter events, 6.7 us)
Async XLA Ops:
  6.5 169.2 %all-gather.2.cloned.1.call-start = ((), (), s32[]{:S(2)}) async-start(), calls=%async_computation | async-start | bytes 20889600 | tf_op jit(solution)/shard_map/all_gather | solution.py:489
  43.5 2.8 %copy-start.14 = (s32[768]{0:T(1024)S(1)}, s32[768]{0:T(1024)}, u32[]{:S(2)}) copy-start(s32[768]{0:T(1024)} %param.28) | copy-start | bytes 9220
  44.4 22.7 %copy-start.19 = (s32[8]{0:T(128)S(1)}, s32[8]{0:T(128)}, u32[]{:S(2)}) copy-start(s32[8]{0:T(128)} %constant.50.clone) | copy-start | bytes 100
  44.4 22.8 %copy-start.20 = (s32[8]{0:T(128)S(1)}, s32[8]{0:T(128)}, u32[]{:S(2)}) copy-start(s32[8]{0:T(128)} %constant.51.clone) | copy-start | bytes 100
  44.4 23.3 %copy-start.8 = (bf16[768,192]{0,1:T(8,128)(2,1)S(1)}, bf16[768,192]{0,1:T(8,128)(2,1)}, u32[]{:S(2)}) copy-start(bf16[768,192]{0,1:T(8,128)(2,1)} %param.22) | copy-start | bytes 884740
  45.3 23.3 %copy-start.9 = (bf16[768,192]{0,1:T(8,128)(2,1)S(1)}, bf16[768,192]{0,1:T(8,128)(2,1)}, u32[]{:S(2)}) copy-start(bf16[768,192]{0,1:T(8,128)(2,1)} %param.25) | copy-start | bytes 884740
  50.5 22.8 %collective-permute-start = (bf16[112,192]{1,0:T(8,128)(2,1)}, bf16[112,192]{1,0:T(8,128)(2,1)S(1)}, u32[]{:S(2)}, u32[]{:S(2)}) collective-permute-start(bf16[112,192]{1,0:T(8,128)(2,1)} %get-tuple-element.24), channel_id=1, source_target_pairs={{0,8},{8,16},{16,24},{24,32},{32,40},{40,48},{48,56},{56,64},{64,7... | collective-permute-start | bytes 129032 | tf_op jit(solution)/shard_map/ppermute | solution.py:514
  54.0 19.3 %collective-permute-start.1 = (bf16[112,192]{1,0:T(8,128)(2,1)}, bf16[112,192]{1,0:T(8,128)(2,1)S(1)}, u32[]{:S(2)}, u32[]{:S(2)}) collective-permute-start(bf16[112,192]{1,0:T(8,128)(2,1)} %get-tuple-element.24), channel_id=1, source_target_pairs={{0,16},{8,24},{16,32},{24,40},{32,48},{40,56},{48,64},{56,72},{64,... | collective-permute-start | bytes 129032 | tf_op jit(solution)/shard_map/ppermute | solution.py:514
  58.6 14.7 %collective-permute-start.2 = (bf16[112,192]{1,0:T(8,128)(2,1)}, bf16[112,192]{1,0:T(8,128)(2,1)S(1)}, u32[]{:S(2)}, u32[]{:S(2)}) collective-permute-start(bf16[112,192]{1,0:T(8,128)(2,1)} %get-tuple-element.24), channel_id=1, source_target_pairs={{0,24},{8,32},{16,40},{24,48},{32,56},{40,64},{48,72},{56,80},{64,... | collective-permute-start | bytes 129032 | tf_op jit(solution)/shard_map/ppermute | solution.py:514
  63.3 10.0 %collective-permute-start.3 = (bf16[112,192]{1,0:T(8,128)(2,1)}, bf16[112,192]{1,0:T(8,128)(2,1)S(1)}, u32[]{:S(2)}, u32[]{:S(2)}) collective-permute-start(bf16[112,192]{1,0:T(8,128)(2,1)} %get-tuple-element.24), channel_id=1, source_target_pairs={{0,32},{8,40},{16,48},{24,56},{32,64},{40,72},{48,80},{56,88},{64,... | collective-permute-start | bytes 129032 | tf_op jit(solution)/shard_map/ppermute | solution.py:514
  81.9 2.0 copy-start.4
  83.4 4.6 %copy-start.3 = (bf16[4,768,384]{2,1,0:T(8,128)(2,1)S(1)}, bf16[4,768,384]{2,1,0:T(8,128)(2,1)}, u32[]{:S(2)}) copy-start(bf16[4,768,384]{2,1,0:T(8,128)(2,1)} %get-tuple-element.25) | copy-start | bytes 7077892
  83.4 8.0 %collective-permute-start.5 = (bf16[2,768,384]{2,1,0:T(8,128)(2,1)S(1)}, bf16[2,768,384]{2,1,0:T(8,128)(2,1)S(1)}, u32[]{:S(2)}, u32[]{:S(2)}) collective-permute-start(bf16[2,768,384]{2,1,0:T(8,128)(2,1)S(1)} %slice.99), channel_id=1, source_target_pairs={{0,1},{1,0},{2,3},{3,2},{4,5},{5,4},{6,7},{7,6},{8,9},{9,8},{10,11... | collective-permute-start | bytes 3538952 | tf_op jit(solution)/shard_map/ppermute | solution.py:419
  84.0 3.2 %collective-permute-start.4 = (bf16[768,384]{1,0:T(8,128)(2,1)S(1)}, bf16[768,384]{1,0:T(8,128)(2,1)S(1)}, u32[]{:S(2)}, u32[]{:S(2)}) collective-permute-start(bf16[768,384]{1,0:T(8,128)(2,1)S(1)} %get-tuple-element.44), channel_id=1, source_target_pairs={{0,1},{1,0},{2,3},{3,2},{4,5},{5,4},{6,7},{7,6},{8,9},{9,8},{10,11... | collective-permute-start | bytes 1769480 | tf_op jit(solution)/shard_map/ppermute | solution.py:419
  84.2 3.8 %collective-permute-start.6 = (bf16[768,384]{1,0:T(8,128)(2,1)S(1)}, bf16[768,384]{1,0:T(8,128)(2,1)S(1)}, u32[]{:S(2)}, u32[]{:S(2)}) collective-permute-start(bf16[768,384]{1,0:T(8,128)(2,1)S(1)} %get-tuple-element.43), channel_id=1, source_target_pairs={{0,1},{1,0},{2,3},{3,2},{4,5},{5,4},{6,7},{7,6},{8,9},{9,8},{10,11... | collective-permute-start | bytes 1769480 | tf_op jit(solution)/shard_map/ppermute | solution.py:419
  88.4 9.6 %collective-permute-start.11 = (bf16[384,384]{1,0:T(8,128)(2,1)S(1)}, bf16[384,384]{1,0:T(8,128)(2,1)S(1)}, u32[]{:S(2)}, u32[]{:S(2)}) collective-permute-start(bf16[384,384]{1,0:T(8,128)(2,1)S(1)} %get-tuple-element.52), channel_id=1, source_target_pairs={{0,6},{2,0},{4,2},{6,4},{1,7},{3,1},{5,3},{7,5},{8,14},{10,8},{12,... | collective-permute-start | bytes 884744 | tf_op jit(solution)/shard_map/ppermute | solution.py:415
  91.4 10.5 %collective-permute-start.7 = (bf16[384,384]{1,0:T(8,128)(2,1)S(1)}, bf16[384,384]{1,0:T(8,128)(2,1)S(1)}, u32[]{:S(2)}, u32[]{:S(2)}) collective-permute-start(bf16[384,384]{1,0:T(8,128)(2,1)S(1)} %get-tuple-element.51), channel_id=1, source_target_pairs={{0,2},{2,4},{4,6},{6,0},{1,3},{3,5},{5,7},{7,1},{8,10},{10,12},{12... | collective-permute-start | bytes 884744 | tf_op jit(solution)/shard_map/ppermute | solution.py:415
  98.1 11.2 %collective-permute-start.12 = (bf16[384,384]{1,0:T(8,128)(2,1)S(1)}, bf16[384,384]{1,0:T(8,128)(2,1)S(1)}, u32[]{:S(2)}, u32[]{:S(2)}) collective-permute-start(bf16[384,384]{1,0:T(8,128)(2,1)S(1)} %fusion.8), channel_id=1, source_target_pairs={{0,6},{2,0},{4,2},{6,4},{1,7},{3,1},{5,3},{7,5},{8,14},{10,8},{12,... | collective-permute-start | bytes 884744 | tf_op jit(solution)/shard_map/ppermute | solution.py:415
  102.0 11.2 %collective-permute-start.8 = (bf16[384,384]{1,0:T(8,128)(2,1)S(1)}, bf16[384,384]{1,0:T(8,128)(2,1)S(1)}, u32[]{:S(2)}, u32[]{:S(2)}) collective-permute-start(bf16[384,384]{1,0:T(8,128)(2,1)S(1)} %fusion.9), channel_id=1, source_target_pairs={{0,2},{2,4},{4,6},{6,0},{1,3},{3,5},{5,7},{7,1},{8,10},{10,12},{12... | collective-permute-start | bytes 884744 | tf_op jit(solution)/shard_map/ppermute | solution.py:415
  102.1 15.5 %collective-permute-start.10 = (bf16[384,384]{1,0:T(8,128)(2,1)S(1)}, bf16[384,384]{1,0:T(8,128)(2,1)S(1)}, u32[]{:S(2)}, u32[]{:S(2)}) collective-permute-start(bf16[384,384]{1,0:T(8,128)(2,1)S(1)} %slice_bitcast_fusion.3), channel_id=1, source_target_pairs={{0,2},{2,4},{4,6},{6,0},{1,3},{3,5},{5,7},{7,1},{8,10},{10,12},{12... | collective-permute-start | bytes 884744 | tf_op jit(solution)/shard_map/ppermute | solution.py:415
  102.2 15.5 %collective-permute-start.9 = (bf16[384,384]{1,0:T(8,128)(2,1)S(1)}, bf16[384,384]{1,0:T(8,128)(2,1)S(1)}, u32[]{:S(2)}, u32[]{:S(2)}) collective-permute-start(bf16[384,384]{1,0:T(8,128)(2,1)S(1)} %slice_bitcast_fusion.4), channel_id=1, source_target_pairs={{0,6},{2,0},{4,2},{6,4},{1,7},{3,1},{5,3},{7,5},{8,14},{10,8},{12,... | collective-permute-start | bytes 884744 | tf_op jit(solution)/shard_map/ppermute | solution.py:415
  118.8 23.2 %slice-start.1 = ((f32[3,1056]{1,0:T(4,128)}), f32[3,32]{1,0:T(4,128)S(1)}, s32[]{:S(2)}) async-start(f32[3,1056]{1,0:T(4,128)} %param.34), calls=%async_computation.2 | async-start | bytes 4096 | tf_op jit(solution)/shard_map/slice | solution.py:496
  118.8 23.2 %copy-start.17 = (s32[8]{0:T(128)S(1)}, s32[8]{0:T(128)}, u32[]{:S(2)}) copy-start(s32[8]{0:T(128)} %constant.52.clone) | copy-start | bytes 100
  118.9 23.2 %copy-start.18 = (s32[8]{0:T(128)S(1)}, s32[8]{0:T(128)}, u32[]{:S(2)}) copy-start(s32[8]{0:T(128)} %constant.53.clone) | copy-start | bytes 100
  118.9 23.2 %copy-start.15 = (s32[8]{0:T(128)S(1)}, s32[8]{0:T(128)}, u32[]{:S(2)}) copy-start(s32[8]{0:T(128)} %constant.54.clone) | copy-start | bytes 100
  118.9 23.2 %copy-start.16 = (s32[8]{0:T(128)S(1)}, s32[8]{0:T(128)}, u32[]{:S(2)}) copy-start(s32[8]{0:T(128)} %constant.55.clone) | copy-start | bytes 100
  118.9 25.1 %copy-start.1 = (f32[3072]{0:T(1024)S(1)}, f32[3072]{0:T(1024)}, u32[]{:S(2)}) copy-start(f32[3072]{0:T(1024)} %param.31) | copy-start | bytes 36868
  118.9 14.9 %collective-permute-start.13 = (bf16[768,384]{1,0:T(8,128)(2,1)S(1)}, bf16[768,384]{1,0:T(8,128)(2,1)S(1)}, u32[]{:S(2)}, u32[]{:S(2)}) collective-permute-start(bf16[768,384]{1,0:T(8,128)(2,1)S(1)} %fusion.3.refs_0_), channel_id=1, source_target_pairs={{0,2},{2,4},{4,6},{6,0},{1,3},{3,5},{5,7},{7,1},{8,10},{10,12},{12... | collective-permute-start | bytes 1769480 | tf_op jit(solution)/shard_map/ppermute | solution.py:415
  119.0 14.9 %collective-permute-start.14 = (bf16[768,384]{1,0:T(8,128)(2,1)S(1)}, bf16[768,384]{1,0:T(8,128)(2,1)S(1)}, u32[]{:S(2)}, u32[]{:S(2)}) collective-permute-start(bf16[768,384]{1,0:T(8,128)(2,1)S(1)} %fusion.3.refs_0_), channel_id=1, source_target_pairs={{0,6},{2,0},{4,2},{6,4},{1,7},{3,1},{5,3},{7,5},{8,14},{10,8},{12,... | collective-permute-start | bytes 1769480 | tf_op jit(solution)/shard_map/ppermute | solution.py:415
  133.8 8.0 %collective-permute-start.15 = (bf16[384,384]{1,0:T(8,128)(2,1)S(1)}, bf16[384,384]{1,0:T(8,128)(2,1)S(1)}, u32[]{:S(2)}, u32[]{:S(2)}) collective-permute-start(bf16[384,384]{1,0:T(8,128)(2,1)S(1)} %slice.136), channel_id=1, source_target_pairs={{0,2},{2,4},{4,6},{6,0},{1,3},{3,5},{5,7},{7,1},{8,10},{10,12},{12... | collective-permute-start | bytes 884744 | tf_op jit(solution)/shard_map/ppermute | solution.py:415
  133.9 7.9 %collective-permute-start.16 = (bf16[384,384]{1,0:T(8,128)(2,1)S(1)}, bf16[384,384]{1,0:T(8,128)(2,1)S(1)}, u32[]{:S(2)}, u32[]{:S(2)}) collective-permute-start(bf16[384,384]{1,0:T(8,128)(2,1)S(1)} %slice.137), channel_id=1, source_target_pairs={{0,6},{2,0},{4,2},{6,4},{1,7},{3,1},{5,3},{7,5},{8,14},{10,8},{12,... | collective-permute-start | bytes 884744 | tf_op jit(solution)/shard_map/ppermute | solution.py:415
  137.2 5.5 %collective-permute-start.17 = (bf16[768,384]{1,0:T(8,128)(2,1)S(1)}, bf16[768,384]{1,0:T(8,128)(2,1)S(1)}, u32[]{:S(2)}, u32[]{:S(2)}) collective-permute-start(bf16[768,384]{1,0:T(8,128)(2,1)S(1)} %fusion.3.refs_0_), channel_id=1, source_target_pairs={{0,1},{1,0},{2,3},{3,2},{4,5},{5,4},{6,7},{7,6},{8,9},{9,8},{10,11... | collective-permute-start | bytes 1769480 | tf_op jit(solution)/shard_map/ppermute | solution.py:419
  137.2 5.5 %collective-permute-start.18 = (bf16[768,384]{1,0:T(8,128)(2,1)S(1)}, bf16[768,384]{1,0:T(8,128)(2,1)S(1)}, u32[]{:S(2)}, u32[]{:S(2)}) collective-permute-start(bf16[768,384]{1,0:T(8,128)(2,1)S(1)} %collective-permute-done.13.refs_1_), channel_id=1, source_target_pairs={{0,1},{1,0},{2,3},{3,2},{4,5},{5,4},{6,7},{7,6},{8,9},{9,8},{10,11... | collective-permute-start | bytes 1769480 | tf_op jit(solution)/shard_map/ppermute | solution.py:419
  137.7 5.0 %collective-permute-start.19 = (bf16[768,384]{1,0:T(8,128)(2,1)S(1)}, bf16[768,384]{1,0:T(8,128)(2,1)S(1)}, u32[]{:S(2)}, u32[]{:S(2)}) collective-permute-start(bf16[768,384]{1,0:T(8,128)(2,1)S(1)} %collective-permute-done.14.refs_2_), channel_id=1, source_target_pairs={{0,1},{1,0},{2,3},{3,2},{4,5},{5,4},{6,7},{7,6},{8,9},{9,8},{10,11... | collective-permute-start | bytes 1769480 | tf_op jit(solution)/shard_map/ppermute | solution.py:419
  141.9 2.1 collective-permute-start.20
  144.0 7.9 %slice-start = ((f32[3,1056]{1,0:T(4,128)}), f32[3,1024]{1,0:T(4,128)S(1)}, s32[]{:S(2)}) async-start(f32[3,1056]{1,0:T(4,128)} %param.34), calls=%async_computation.1 | async-start | bytes 32768 | tf_op jit(solution)/shard_map/slice | solution.py:495
  149.4 7.6 %collective-permute-start.21 = (bf16[16,3072]{1,0:T(8,128)(2,1)S(1)}, bf16[16,3072]{1,0:T(8,128)(2,1)S(1)}, u32[]{:S(2)}, u32[]{:S(2)}) collective-permute-start(bf16[16,3072]{1,0:T(8,128)(2,1)S(1)} %get-tuple-element.28), channel_id=1, source_target_pairs={{0,8},{8,16},{16,24},{24,32},{32,40},{40,48},{48,56},{56,64},{64,7... | collective-permute-start | bytes 294920 | tf_op jit(solution)/shard_map/ppermute | solution.py:586
  200.2 2.3 collective-permute-start.24
  200.3 10.5 %collective-permute-start.23 = (bf16[2,768,384]{2,1,0:T(8,128)(2,1)}, bf16[2,768,384]{2,1,0:T(8,128)(2,1)S(1)}, u32[]{:S(2)}, u32[]{:S(2)}) collective-permute-start(bf16[2,768,384]{2,1,0:T(8,128)(2,1)} %get-tuple-element.34), channel_id=1, source_target_pairs={{0,1},{1,0},{2,3},{3,2},{4,5},{5,4},{6,7},{7,6},{8,9},{9,8},{10,11... | collective-permute-start | bytes 3538952 | tf_op jit(solution)/shard_map/ppermute | solution.py:419
  202.5 4.5 %copy-start = (bf16[768,1152]{1,0:T(8,128)(2,1)S(1)}, bf16[768,1152]{1,0:T(8,128)(2,1)}, u32[]{:S(2)}) copy-start(bf16[768,1152]{1,0:T(8,128)(2,1)} %get-tuple-element.31.h_ref) | copy-start | bytes 5308420
  202.5 4.5 %copy-start.2 = (s32[8]{0:T(128)S(1)}, s32[8]{0:T(128)}, u32[]{:S(2)}) copy-start(s32[8]{0:T(128)} %fusion.15.order_ref) | copy-start | bytes 100
  203.9 10.6 %collective-permute-start.29 = (bf16[384,384]{1,0:T(8,128)(2,1)S(1)}, bf16[384,384]{1,0:T(8,128)(2,1)S(1)}, u32[]{:S(2)}, u32[]{:S(2)}) collective-permute-start(bf16[384,384]{1,0:T(8,128)(2,1)S(1)} %get-tuple-element.50), channel_id=1, source_target_pairs={{0,6},{2,0},{4,2},{6,4},{1,7},{3,1},{5,3},{7,5},{8,14},{10,8},{12,... | collective-permute-start | bytes 884744 | tf_op jit(solution)/shard_map/ppermute | solution.py:415
  210.6 14.1 %collective-permute-start.22 = (bf16[768,384]{1,0:T(8,128)(2,1)S(1)}, bf16[768,384]{1,0:T(8,128)(2,1)S(1)}, u32[]{:S(2)}, u32[]{:S(2)}) collective-permute-start(bf16[768,384]{1,0:T(8,128)(2,1)S(1)} %get-tuple-element.33), channel_id=1, source_target_pairs={{0,1},{1,0},{2,3},{3,2},{4,5},{5,4},{6,7},{7,6},{8,9},{9,8},{10,11... | collective-permute-start | bytes 1769480 | tf_op jit(solution)/shard_map/ppermute | solution.py:419
  210.7 10.6 %collective-permute-start.25 = (bf16[384,384]{1,0:T(8,128)(2,1)S(1)}, bf16[384,384]{1,0:T(8,128)(2,1)S(1)}, u32[]{:S(2)}, u32[]{:S(2)}) collective-permute-start(bf16[384,384]{1,0:T(8,128)(2,1)S(1)} %get-tuple-element.49), channel_id=1, source_target_pairs={{0,2},{2,4},{4,6},{6,0},{1,3},{3,5},{5,7},{7,1},{8,10},{10,12},{12... | collective-permute-start | bytes 884744 | tf_op jit(solution)/shard_map/ppermute | solution.py:415
  214.6 10.2 %collective-permute-start.30 = (bf16[384,384]{1,0:T(8,128)(2,1)S(1)}, bf16[384,384]{1,0:T(8,128)(2,1)S(1)}, u32[]{:S(2)}, u32[]{:S(2)}) collective-permute-start(bf16[384,384]{1,0:T(8,128)(2,1)S(1)} %add_convert_fusion.2), channel_id=1, source_target_pairs={{0,6},{2,0},{4,2},{6,4},{1,7},{3,1},{5,3},{7,5},{8,14},{10,8},{12,... | collective-permute-start | bytes 884744 | tf_op jit(solution)/shard_map/ppermute | solution.py:415
  221.4 11.2 %collective-permute-start.26 = (bf16[384,384]{1,0:T(8,128)(2,1)S(1)}, bf16[384,384]{1,0:T(8,128)(2,1)S(1)}, u32[]{:S(2)}, u32[]{:S(2)}) collective-permute-start(bf16[384,384]{1,0:T(8,128)(2,1)S(1)} %add_convert_fusion.3), channel_id=1, source_target_pairs={{0,2},{2,4},{4,6},{6,0},{1,3},{3,5},{5,7},{7,1},{8,10},{10,12},{12... | collective-permute-start | bytes 884744 | tf_op jit(solution)/shard_map/ppermute | solution.py:415
  221.5 11.1 %collective-permute-start.27 = (bf16[384,384]{1,0:T(8,128)(2,1)S(1)}, bf16[384,384]{1,0:T(8,128)(2,1)S(1)}, u32[]{:S(2)}, u32[]{:S(2)}) collective-permute-start(bf16[384,384]{1,0:T(8,128)(2,1)S(1)} %slice.121), channel_id=1, source_target_pairs={{0,6},{2,0},{4,2},{6,4},{1,7},{3,1},{5,3},{7,5},{8,14},{10,8},{12,... | collective-permute-start | bytes 884744 | tf_op jit(solution)/shard_map/ppermute | solution.py:415
  224.7 12.8 %collective-permute-start.28 = (bf16[384,384]{1,0:T(8,128)(2,1)S(1)}, bf16[384,384]{1,0:T(8,128)(2,1)S(1)}, u32[]{:S(2)}, u32[]{:S(2)}) collective-permute-start(bf16[384,384]{1,0:T(8,128)(2,1)S(1)} %slice.123), channel_id=1, source_target_pairs={{0,2},{2,4},{4,6},{6,0},{1,3},{3,5},{5,7},{7,1},{8,10},{10,12},{12... | collective-permute-start | bytes 884744 | tf_op jit(solution)/shard_map/ppermute | solution.py:415
  (7 other events, 6.5 us)
Sparse Core Ops, SparseCore 0:
  43.6 132.0 all-gather.1

commit v2 on v0

--- a/solution.py
+++ b/solution.py
@@ -213,6 +213,7 @@
     wt_ref,
     w_ref,
     h_ref,
+    far_swap_ref,
     swap_ref,
     own_ref,
     gate_scr,
@@ -329,7 +330,7 @@
                 copy.wait()
         known = main - tile
         both = product(0, (slice(0, known), slice(main, main + 128), slice(known, main)))
-        swap_ref[0], own_ref[0] = both[:, :cols], both[:, cols:]
+        far_swap_ref[0], own_ref[0] = both[:, :cols], both[:, cols:]
 
     @pl.when(j > tiles)
     def _():
@@ -337,7 +338,7 @@
             for copy in copies(n):
                 copy.wait()
         both = product(1, (slice(None),))
-        swap_ref[1], swap_ref[2] = both[:, :cols], both[:, cols:]
+        swap_ref[0], swap_ref[1] = both[:, :cols], both[:, cols:]
 
 
 def two_parts(h_ref, wa_ref, wb_ref, ta_ref, tb_ref):
@@ -380,9 +381,10 @@
     return lax.ppermute(value, "c", [(0, 1), (1, 0)])
 
 
-def summed_over_tp(swap, own, sides, last):
+def summed_over_tp(far_swap, swap, own, sides, last):
+    far_swap = swapped(far_swap)
     other = swapped(swap)
-    far = added(own, other[0]).astype(BF16)
+    far = added(own, far_swap).astype(BF16)
     half = far.shape[0] // 2
     far_up, far_down = shifted(far[:half], 1), shifted(far[half:], -1)
     up, down = sides(other)
@@ -436,6 +438,9 @@
     spare = hidden - main
     packed = pl.pallas_call(
         pack_kernel,
+        grid=(3,),
+        in_specs=[pl.BlockSpec((w_gate.shape[0] // 3, hidden), lambda i: (i, 0))] * 3,
+        out_specs=pl.BlockSpec((w_gate.shape[0] // 3, 3 * main + 128), lambda i: (i, 0)),
         out_shape=shape((w_gate.shape[0], 3 * main + 128), BF16),
         name="pack",
     )(w_gate, w_value, w_down.T)
@@ -509,9 +514,10 @@
         name="mix",
     )(order, query, out_gate, local, rows, cols_aux, head_gain.reshape(1, width), w_out, w_out, *pays)
     attended = summed_over_tp(
-        swap[:3],
+        swap[0],
+        swap[1:3],
         own[0],
-        lambda other: tuple(added(own[k], other[k]).astype(BF16) for k in (1, 2)),
+        lambda other: tuple(added(own[1 + k], other[k]).astype(BF16) for k in range(2)),
         lambda: (swap[3], own[3]),
     )
     residual_own = resid.astype(F32) + jnp.concatenate(attended, axis=0)
@@ -541,7 +547,7 @@
     order = (chip + jnp.array([2, 2, 1, 3, 1, 3, 0, 0], jnp.int32)) % ring * cores + (
         core ^ jnp.array([1, 0, 1, 1, 0, 0, 1, 0], jnp.int32)
     )
-    hidden, swap, own = pl.pallas_call(
+    hidden, far_swap, swap, own = pl.pallas_call(
         mixer_kernel,
         grid_spec=pltpu.PrefetchScalarGridSpec(
             num_scalar_prefetch=1,
@@ -564,7 +570,8 @@
             ],
             out_specs=(
                 whole((tokens, main + 128)),
-                whole((3, tokens, cols)),
+                whole((1, tokens, cols)),
+                whole((2, tokens, cols)),
                 whole((1, tokens, cols)),
             ),
             scratch_shapes=[
@@ -577,7 +584,8 @@
         ),
         out_shape=(
             shape((tokens, main + 128), BF16),
-            shape((3, tokens, cols), BF16),
+            shape((1, tokens, cols), BF16),
+            shape((2, tokens, cols), BF16),
             shape((1, tokens, cols), BF16),
         ),
         compiler_params=pltpu.CompilerParams(vmem_limit_bytes=58 * 2**20),
@@ -609,13 +617,14 @@
         )(order, hidden, *[weights] * 4, *given)
 
     down = summed_over_tp(
+        far_swap[0],
         swap,
         own[0],
         lambda other: more(
             side_kernel,
             4,
             (other, other),
-            [pl.BlockSpec((1, tokens, cols), lambda j, order, k=k: (k, 0, 0)) for k in (1, 2)],
+            [pl.BlockSpec((1, tokens, cols), lambda j, order, k=k: (k, 0, 0)) for k in (0, 1)],
         ),
         lambda: more(down_kernel, 6, (), []),
     )

time: 210 us -> 212 us (level)
    ppermute x16, waiting for transfers between devices: 44.6 us -> 50.2 us  [shifted(): return lax.ppermute(value, 'y', [(i, (i + by) % ring) for i in range(ring)])]
    all_gather x1, waiting for transfers between devices: 22.1 us -> 18.2 us  [layer(): weights = lax.all_gather(packed, SP, axis=0, tiled=True)]
    unnamed x45 -> x47, local copies, waits for them, and re-layouts: 5.35 us -> 6.65 us
    ppermute x8 -> x10, waiting for transfers between devices: 7.2 us -> 6.47 us  [swapped(): return lax.ppermute(value, 'c', [(0, 1), (1, 0)])]
  transfers between devices with their start and end apart: 30 -> 32, of which waited for: 16 -> 15; matrix products, arithmetic and copies ran while one was open for 5% -> 5% of each run, Pallas kernels for 13% -> 13%
where the time goes in v2:
time: 212 us
  waiting for transfers between devices  79.2 us (37%)
  Pallas kernels  55.3 us (26%)
  starting transfers between devices  47.7 us (22%)
  between operations  13.9 us (7%)
  local copies, waits for them, and re-layouts  9.97 us (5%)
  other arithmetic  5.52 us (3%)
    ppermute x16, waiting for transfers between devices, shifted(): return lax.ppermute(value, 'y', [(i, (i + by) % ring) for i in range(ring)])  50.2 us
    ppermute x16, starting transfers between devices, shifted(): return lax.ppermute(value, 'y', [(i, (i + by) % ring) for i in range(ring)])  26.5 us
    pallas_call x1, Pallas kernels, layer(): pl.pallas_call(mixer_kernel, grid_spec=pltpu.PrefetchScalarGridSpec(num_s...  24.1 us
    all_gather x1, waiting for transfers between devices, layer(): weights = lax.all_gather(packed, SP, axis=0, tiled=True)  18.2 us
    ppermute x4, starting transfers between devices, layer(): lax.ppermute(pay, SP, [(i, i + k) for i in range(count - k)])  16.7 us
    pallas_call x1, Pallas kernels, layer(): pl.pallas_call(mix_kernel, grid_spec=pltpu.PrefetchScalarGridSpec(num_sca...  7.95 us
    pallas_call x2, Pallas kernels, more(): pl.pallas_call(kernel, grid_spec=pltpu.PrefetchScalarGridSpec(num_scalar_...  7.31 us
    unnamed x47, local copies, waits for them, and re-layouts  6.65 us
  transfers between devices with their start and end apart: 32, of which 15 were waited for; matrix products, arithmetic and copies ran while one was open for 5% of the time, Pallas kernels for 13%

profile of v2, /device:TPU:0, one launch (start us, length us, event | category | flops | bytes accessed | tf_op | source)
XLA Modules:
  0.0 211.6 jit_solution(7328401345764091890)
XLA Ops:
  6.5 3.3 %pack.1 = bf16[192,3200]{1,0:T(8,128)(2,1)} custom-call(bf16[192,1056]{1,0:T(8,128)(2,1)} %gate_ref.2, bf16[192,1056]{1,0:T(8,128)(2,1)} %value_ref.1, bf16[192,1056]{1,0:T(8,128)(2,1)} %bitcast.37), custom_call_target="tpu_custom_call" | custom-call | tf_op jit(solution)/shard_map/pack/pallas_call | solution.py:439
  9.9 0.9 copy-done.6
  10.8 0.9 copy.25.k_ref
  11.8 0.9 copy.26.v_ref
  12.7 0.6 reshape.34.doc_ref
  13.3 3.6 %state.1 = (bf16[112,192]{1,0:T(8,128)(2,1)}, f32[8,768]{1,0:T(8,128)}, f32[768,8]{1,0:T(8,128)}) custom-call(bf16[768,192]{1,0:T(8,128)(2,1)} %copy.25.k_ref, bf16[768,192]{1,0:T(8,128)(2,1)} %copy.26.v_ref, f32[2,768]{1,0:T(2,128)} %in_ref.1, f32[2,768]{1,0:T(2,128)} %forget_ref.1, s32[1,768]{1,0:T(1,128)} %reshape.34.doc_ref), custom_call_target="tpu_custom_call" | custom-call | tf_op jit(solution)/shard_map/state/pallas_call | solution.py:459
  16.9 3.5 %collective-permute-start = (bf16[112,192]{1,0:T(8,128)(2,1)}, bf16[112,192]{1,0:T(8,128)(2,1)S(1)}, u32[]{:S(2)}, u32[]{:S(2)}) collective-permute-start(bf16[112,192]{1,0:T(8,128)(2,1)} %get-tuple-element.24), channel_id=1, source_target_pairs={{0,8},{8,16},{16,24},{24,32},{32,40},{40,48},{48,56},{56,64},{64,7... | collective-permute-start | bytes 129032 | tf_op jit(solution)/shard_map/ppermute | solution.py:472
  20.4 4.6 %collective-permute-start.1 = (bf16[112,192]{1,0:T(8,128)(2,1)}, bf16[112,192]{1,0:T(8,128)(2,1)S(1)}, u32[]{:S(2)}, u32[]{:S(2)}) collective-permute-start(bf16[112,192]{1,0:T(8,128)(2,1)} %get-tuple-element.24), channel_id=1, source_target_pairs={{0,16},{8,24},{16,32},{24,40},{32,48},{40,56},{48,64},{56,72},{64,... | collective-permute-start | bytes 129032 | tf_op jit(solution)/shard_map/ppermute | solution.py:472
  25.0 4.7 %collective-permute-start.2 = (bf16[112,192]{1,0:T(8,128)(2,1)}, bf16[112,192]{1,0:T(8,128)(2,1)S(1)}, u32[]{:S(2)}, u32[]{:S(2)}) collective-permute-start(bf16[112,192]{1,0:T(8,128)(2,1)} %get-tuple-element.24), channel_id=1, source_target_pairs={{0,24},{8,32},{16,40},{24,48},{32,56},{40,64},{48,72},{56,80},{64,... | collective-permute-start | bytes 129032 | tf_op jit(solution)/shard_map/ppermute | solution.py:472
  29.7 3.8 %collective-permute-start.3 = (bf16[112,192]{1,0:T(8,128)(2,1)}, bf16[112,192]{1,0:T(8,128)(2,1)S(1)}, u32[]{:S(2)}, u32[]{:S(2)}) collective-permute-start(bf16[112,192]{1,0:T(8,128)(2,1)} %get-tuple-element.24), channel_id=1, source_target_pairs={{0,32},{8,40},{16,48},{24,56},{32,64},{40,72},{48,80},{56,88},{64,... | collective-permute-start | bytes 129032 | tf_op jit(solution)/shard_map/ppermute | solution.py:472
  34.2 0.9 copy.27.q_ref
  35.1 0.9 copy.28.gate_ref
  36.0 3.7 %local.1.local_ref = f32[768,192]{1,0:T(8,128)} custom-call(bf16[768,192]{1,0:T(8,128)(2,1)} %copy.27.q_ref, bf16[768,192]{1,0:T(8,128)(2,1)} %copy.25.k_ref, bf16[768,192]{1,0:T(8,128)(2,1)} %copy.26.v_ref, f32[8,768]{1,0:T(8,128)} %get-tuple-element.22.row_ref, f32[768,8]{1,0:T(8,128)} %get-tuple-element.23.col_ref), custom_call_target="tpu_custom_call" | custom-call | tf_op jit(solution)/shard_map/local/pallas_call | solution.py:474
  40.4 7.9 %mix.1 = (bf16[4,768,384]{2,1,0:T(8,128)(2,1)}, bf16[4,768,384]{2,1,0:T(8,128)(2,1)}, f32[768,128]{1,0:T(8,128)}, f32[768,128]{1,0:T(8,128)}) custom-call(s32[8]{0:T(128)} %fusion.12.order_ref, bf16[768,192]{1,0:T(8,128)(2,1)} %copy.27.q_ref, bf16[768,192]{1,0:T(8,128)(2,1)} %copy.28.gate_ref, f32[768,192]{1,0:T(8,128)} %local.1.local_ref, ...), custom_call_target="tpu_custom_call" | custom-call | tf_op jit(solution)/shard_map/mix/pallas_call | solution.py:484
  48.3 1.5 slice.99
  51.0 2.6 %collective-permute-done.4 = bf16[768,384]{1,0:T(8,128)(2,1)S(1)} collective-permute-done((bf16[768,384]{1,0:T(8,128)(2,1)S(1)}, bf16[768,384]{1,0:T(8,128)(2,1)S(1)}, u32[]{:S(2)}, u32[]{:S(2)}) %collective-permute-start.4) | collective-permute-done | bytes 589856 | tf_op jit(solution)/shard_map/ppermute | solution.py:381
  53.6 0.8 collective-permute-done.6
  54.8 3.0 %collective-permute-start.11 = (bf16[384,384]{1,0:T(8,128)(2,1)S(1)}, bf16[384,384]{1,0:T(8,128)(2,1)S(1)}, u32[]{:S(2)}, u32[]{:S(2)}) collective-permute-start(bf16[384,384]{1,0:T(8,128)(2,1)S(1)} %get-tuple-element.52), channel_id=1, source_target_pairs={{0,6},{2,0},{4,2},{6,4},{1,7},{3,1},{5,3},{7,5},{8,14},{10,8},{12,... | collective-permute-start | bytes 884744 | tf_op jit(solution)/shard_map/ppermute | solution.py:377
  58.2 6.2 %collective-permute-done.11 = bf16[384,384]{1,0:T(8,128)(2,1)S(1)} collective-permute-done((bf16[384,384]{1,0:T(8,128)(2,1)S(1)}, bf16[384,384]{1,0:T(8,128)(2,1)S(1)}, u32[]{:S(2)}, u32[]{:S(2)}) %collective-permute-start.11) | collective-permute-done | bytes 294944 | tf_op jit(solution)/shard_map/ppermute | solution.py:377
  64.5 3.8 %collective-permute-start.12 = (bf16[384,384]{1,0:T(8,128)(2,1)S(1)}, bf16[384,384]{1,0:T(8,128)(2,1)S(1)}, u32[]{:S(2)}, u32[]{:S(2)}) collective-permute-start(bf16[384,384]{1,0:T(8,128)(2,1)S(1)} %fusion.8), channel_id=1, source_target_pairs={{0,6},{2,0},{4,2},{6,4},{1,7},{3,1},{5,3},{7,5},{8,14},{10,8},{12,... | collective-permute-start | bytes 884744 | tf_op jit(solution)/shard_map/ppermute | solution.py:377
  68.6 3.2 %collective-permute-start.9 = (bf16[384,384]{1,0:T(8,128)(2,1)S(1)}, bf16[384,384]{1,0:T(8,128)(2,1)S(1)}, u32[]{:S(2)}, u32[]{:S(2)}) collective-permute-start(bf16[384,384]{1,0:T(8,128)(2,1)S(1)} %slice_bitcast_fusion.4), channel_id=1, source_target_pairs={{0,6},{2,0},{4,2},{6,4},{1,7},{3,1},{5,3},{7,5},{8,14},{10,8},{12,... | collective-permute-start | bytes 884744 | tf_op jit(solution)/shard_map/ppermute | solution.py:377
  71.8 3.9 %collective-permute-done.12 = bf16[384,384]{1,0:T(8,128)(2,1)S(1)} collective-permute-done((bf16[384,384]{1,0:T(8,128)(2,1)S(1)}, bf16[384,384]{1,0:T(8,128)(2,1)S(1)}, u32[]{:S(2)}, u32[]{:S(2)}) %collective-permute-start.12) | collective-permute-done | bytes 294944 | tf_op jit(solution)/shard_map/ppermute | solution.py:377
  75.7 3.9 %collective-permute-done.8 = bf16[384,384]{1,0:T(8,128)(2,1)S(1)} collective-permute-done((bf16[384,384]{1,0:T(8,128)(2,1)S(1)}, bf16[384,384]{1,0:T(8,128)(2,1)S(1)}, u32[]{:S(2)}, u32[]{:S(2)}) %collective-permute-start.8) | collective-permute-done | bytes 294944 | tf_op jit(solution)/shard_map/ppermute | solution.py:377
  79.6 4.5 %collective-permute-done.10 = bf16[384,384]{1,0:T(8,128)(2,1)S(1)} collective-permute-done((bf16[384,384]{1,0:T(8,128)(2,1)S(1)}, bf16[384,384]{1,0:T(8,128)(2,1)S(1)}, u32[]{:S(2)}, u32[]{:S(2)}) %collective-permute-start.10) | collective-permute-done | bytes 294944 | tf_op jit(solution)/shard_map/ppermute | solution.py:377
  84.2 0.9 copy-done.5
  85.4 3.2 %collective-permute-start.14 = (bf16[768,384]{1,0:T(8,128)(2,1)S(1)}, bf16[768,384]{1,0:T(8,128)(2,1)S(1)}, u32[]{:S(2)}, u32[]{:S(2)}) collective-permute-start(bf16[768,384]{1,0:T(8,128)(2,1)S(1)} %fusion.3.refs_0_), channel_id=1, source_target_pairs={{0,6},{2,0},{4,2},{6,4},{1,7},{3,1},{5,3},{7,5},{8,14},{10,8},{12,... | collective-permute-start | bytes 1769480 | tf_op jit(solution)/shard_map/ppermute | solution.py:377
  88.6 11.6 %collective-permute-done.13.refs_1_ = bf16[768,384]{1,0:T(8,128)(2,1)S(1)} collective-permute-done((bf16[768,384]{1,0:T(8,128)(2,1)S(1)}, bf16[768,384]{1,0:T(8,128)(2,1)S(1)}, u32[]{:S(2)}, u32[]{:S(2)}) %collective-permute-start.13) | collective-permute-done | bytes 589856 | tf_op jit(solution)/shard_map/ppermute | solution.py:377
  100.4 3.3 %collective-permute-start.16 = (bf16[384,384]{1,0:T(8,128)(2,1)S(1)}, bf16[384,384]{1,0:T(8,128)(2,1)S(1)}, u32[]{:S(2)}, u32[]{:S(2)}) collective-permute-start(bf16[384,384]{1,0:T(8,128)(2,1)S(1)} %slice.137), channel_id=1, source_target_pairs={{0,6},{2,0},{4,2},{6,4},{1,7},{3,1},{5,3},{7,5},{8,14},{10,8},{12,... | collective-permute-start | bytes 884744 | tf_op jit(solution)/shard_map/ppermute | solution.py:377
  104.2 4.1 %collective-permute-done.15 = bf16[384,384]{1,0:T(8,128)(2,1)S(1)} collective-permute-done((bf16[384,384]{1,0:T(8,128)(2,1)S(1)}, bf16[384,384]{1,0:T(8,128)(2,1)S(1)}, u32[]{:S(2)}, u32[]{:S(2)}) %collective-permute-start.15) | collective-permute-done | bytes 294944 | tf_op jit(solution)/shard_map/ppermute | solution.py:377
  109.1 1.3 collective-permute-done.20.refs_7_
  110.4 5.3 %norm.1 = (bf16[784,3072]{1,0:T(8,128)(2,1)}, bf16[16,3072]{1,0:T(8,128)(2,1)S(1)}) custom-call(s32[8]{0:T(128)S(1)} %fusion.18.order_ref, bf16[768,384]{1,0:T(8,128)(2,1)S(1)} %fusion.3.refs_0_, bf16[768,384]{1,0:T(8,128)(2,1)S(1)} %collective-permute-done.13.refs_1_, bf16[768,384]{1,0:T(8,128)(2,1)S(1)} %collective-permute-done.14.refs_2_, ...), custom_call_target="tpu_custom_call" | custom-call | tf_op jit(solution)/shard_map/norm/pallas_call | solution.py:529
  115.8 2.6 %collective-permute-start.21 = (bf16[16,3072]{1,0:T(8,128)(2,1)S(1)}, bf16[16,3072]{1,0:T(8,128)(2,1)S(1)}, u32[]{:S(2)}, u32[]{:S(2)}) collective-permute-start(bf16[16,3072]{1,0:T(8,128)(2,1)S(1)} %get-tuple-element.28), channel_id=1, source_target_pairs={{0,8},{8,16},{16,24},{24,32},{32,40},{40,48},{48,56},{56,64},{64,7... | collective-permute-start | bytes 294920 | tf_op jit(solution)/shard_map/ppermute | solution.py:544
  118.3 0.6 pad_maximum_fusion.taps_ref
  119.0 4.4 %collective-permute-done.21 = bf16[16,3072]{1,0:T(8,128)(2,1)S(1)} collective-permute-done((bf16[16,3072]{1,0:T(8,128)(2,1)S(1)}, bf16[16,3072]{1,0:T(8,128)(2,1)S(1)}, u32[]{:S(2)}, u32[]{:S(2)}) %collective-permute-start.21) | collective-permute-done | bytes 98336 | tf_op jit(solution)/shard_map/ppermute | solution.py:544
  123.4 0.6 constant_dynamic-update-slice_fusion.2.x_ref
  124.0 18.2 %all-gather.2.cloned.1.call-done.wg_ref.wv_ref.wt_ref.w_ref.wa_ref.wb_ref.ta_ref.tb_ref = bf16[3072,3200]{1,0:T(8,128)(2,1)} async-done(((bf16[192,3200]{1,0:T(8,128)(2,1)}), bf16[3072,3200]{1,0:T(8,128)(2,1)}) %all-gather.2.cloned.1.call-update) | async-done | bytes 19660816 | tf_op jit(solution)/shard_map/all_gather | solution.py:447
  142.2 24.1 %mixer.1 = (bf16[768,1152]{1,0:T(8,128)(2,1)}, bf16[1,768,384]{2,1,0:T(8,128)(2,1)}, bf16[2,768,384]{2,1,0:T(8,128)(2,1)}, bf16[1,768,384]{2,1,0:T(8,128)(2,1)}) custom-call(s32[8]{0:T(128)} %fusion.15.order_ref, bf16[784,3072]{1,0:T(8,128)(2,1)} %constant_dynamic-update-slice_fusion.2.x_ref, f32[768,128]{1,0:T(8,128)} %get-tuple-element.29.near_ref, ...), custom_call_target="tpu_custom_call" | custom-call | tf_op jit(solution)/shard_map/mixer/pallas_call | solution.py:550
  166.8 1.7 collective-permute-done.24
  168.5 1.3 fusion.1
  169.9 3.0 %collective-permute-start.29 = (bf16[384,384]{1,0:T(8,128)(2,1)S(1)}, bf16[384,384]{1,0:T(8,128)(2,1)S(1)}, u32[]{:S(2)}, u32[]{:S(2)}) collective-permute-start(bf16[384,384]{1,0:T(8,128)(2,1)S(1)} %get-tuple-element.50), channel_id=1, source_target_pairs={{0,6},{2,0},{4,2},{6,4},{1,7},{3,1},{5,3},{7,5},{8,14},{10,8},{12,... | collective-permute-start | bytes 884744 | tf_op jit(solution)/shard_map/ppermute | solution.py:377
  173.0 3.6 %shard_map.199 = (bf16[768,384]{1,0:T(8,128)(2,1)S(1)}, bf16[768,384]{1,0:T(8,128)(2,1)S(1)}) custom-call(s32[8]{0:T(128)S(1)} %copy-done.2, bf16[768,1152]{1,0:T(8,128)(2,1)S(1)} %copy-done, bf16[3072,3200]{1,0:T(8,128)(2,1)} %all-gather.2.cloned.1.call-done.wg_ref.wv_ref.wt_ref.w_ref.wa_ref.wb_ref.ta_ref.tb_ref, ...), custom_call_target="tpu_custom_call" | custom-call | tf_op jit(solution)/shard_map/pallas_call | solution.py:600
  176.8 3.7 %shard_map.200 = (bf16[768,384]{1,0:T(8,128)(2,1)S(1)}, bf16[768,384]{1,0:T(8,128)(2,1)S(1)}) custom-call(s32[8]{0:T(128)S(1)} %copy-done.2, bf16[768,1152]{1,0:T(8,128)(2,1)S(1)} %copy-done, bf16[3072,3200]{1,0:T(8,128)(2,1)} %all-gather.2.cloned.1.call-done.wg_ref.wv_ref.wt_ref.w_ref.wa_ref.wb_ref.ta_ref.tb_ref, ...), custom_call_target="tpu_custom_call" | custom-call | tf_op jit(solution)/shard_map/pallas_call | solution.py:600
  180.6 3.3 %collective-permute-start.30 = (bf16[384,384]{1,0:T(8,128)(2,1)S(1)}, bf16[384,384]{1,0:T(8,128)(2,1)S(1)}, u32[]{:S(2)}, u32[]{:S(2)}) collective-permute-start(bf16[384,384]{1,0:T(8,128)(2,1)S(1)} %add_convert_fusion.2), channel_id=1, source_target_pairs={{0,6},{2,0},{4,2},{6,4},{1,7},{3,1},{5,3},{7,5},{8,14},{10,8},{12,... | collective-permute-start | bytes 884744 | tf_op jit(solution)/shard_map/ppermute | solution.py:377
  183.9 3.4 %collective-permute-done.25 = bf16[384,384]{1,0:T(8,128)(2,1)S(1)} collective-permute-done((bf16[384,384]{1,0:T(8,128)(2,1)S(1)}, bf16[384,384]{1,0:T(8,128)(2,1)S(1)}, u32[]{:S(2)}, u32[]{:S(2)}) %collective-permute-start.25) | collective-permute-done | bytes 294944 | tf_op jit(solution)/shard_map/ppermute | solution.py:377
  187.5 3.2 %collective-permute-start.27 = (bf16[384,384]{1,0:T(8,128)(2,1)S(1)}, bf16[384,384]{1,0:T(8,128)(2,1)S(1)}, u32[]{:S(2)}, u32[]{:S(2)}) collective-permute-start(bf16[384,384]{1,0:T(8,128)(2,1)S(1)} %slice.121), channel_id=1, source_target_pairs={{0,6},{2,0},{4,2},{6,4},{1,7},{3,1},{5,3},{7,5},{8,14},{10,8},{12,... | collective-permute-start | bytes 884744 | tf_op jit(solution)/shard_map/ppermute | solution.py:377
  190.9 7.7 %collective-permute-done.26 = bf16[384,384]{1,0:T(8,128)(2,1)S(1)} collective-permute-done((bf16[384,384]{1,0:T(8,128)(2,1)S(1)}, bf16[384,384]{1,0:T(8,128)(2,1)S(1)}, u32[]{:S(2)}, u32[]{:S(2)}) %collective-permute-start.26) | collective-permute-done | bytes 294944 | tf_op jit(solution)/shard_map/ppermute | solution.py:377
  198.6 4.9 %collective-permute-done.28 = bf16[384,384]{1,0:T(8,128)(2,1)S(1)} collective-permute-done((bf16[384,384]{1,0:T(8,128)(2,1)S(1)}, bf16[384,384]{1,0:T(8,128)(2,1)S(1)}, u32[]{:S(2)}, u32[]{:S(2)}) %collective-permute-start.28) | collective-permute-done | bytes 294944 | tf_op jit(solution)/shard_map/ppermute | solution.py:377
  203.7 1.0 fusion
  (106 shorter events, 6.7 us)
Async XLA Ops:
  6.5 135.6 %all-gather.2.cloned.1.call-start = ((), (), s32[]{:S(2)}) async-start(), calls=%async_computation | async-start | bytes 20889600 | tf_op jit(solution)/shard_map/all_gather | solution.py:447
  9.9 2.8 %copy-start.14 = (s32[768]{0:T(1024)S(1)}, s32[768]{0:T(1024)}, u32[]{:S(2)}) copy-start(s32[768]{0:T(1024)} %param.28) | copy-start | bytes 9220
  10.8 22.7 %copy-start.19 = (s32[8]{0:T(128)S(1)}, s32[8]{0:T(128)}, u32[]{:S(2)}) copy-start(s32[8]{0:T(128)} %constant.50.clone) | copy-start | bytes 100
  10.8 22.8 %copy-start.20 = (s32[8]{0:T(128)S(1)}, s32[8]{0:T(128)}, u32[]{:S(2)}) copy-start(s32[8]{0:T(128)} %constant.51.clone) | copy-start | bytes 100
  10.8 23.3 %copy-start.8 = (bf16[768,192]{0,1:T(8,128)(2,1)S(1)}, bf16[768,192]{0,1:T(8,128)(2,1)}, u32[]{:S(2)}) copy-start(bf16[768,192]{0,1:T(8,128)(2,1)} %param.22) | copy-start | bytes 884740
  11.8 23.3 %copy-start.9 = (bf16[768,192]{0,1:T(8,128)(2,1)S(1)}, bf16[768,192]{0,1:T(8,128)(2,1)}, u32[]{:S(2)}) copy-start(bf16[768,192]{0,1:T(8,128)(2,1)} %param.25) | copy-start | bytes 884740
  16.9 22.8 %collective-permute-start = (bf16[112,192]{1,0:T(8,128)(2,1)}, bf16[112,192]{1,0:T(8,128)(2,1)S(1)}, u32[]{:S(2)}, u32[]{:S(2)}) collective-permute-start(bf16[112,192]{1,0:T(8,128)(2,1)} %get-tuple-element.24), channel_id=1, source_target_pairs={{0,8},{8,16},{16,24},{24,32},{32,40},{40,48},{48,56},{56,64},{64,7... | collective-permute-start | bytes 129032 | tf_op jit(solution)/shard_map/ppermute | solution.py:472
  20.4 19.3 %collective-permute-start.1 = (bf16[112,192]{1,0:T(8,128)(2,1)}, bf16[112,192]{1,0:T(8,128)(2,1)S(1)}, u32[]{:S(2)}, u32[]{:S(2)}) collective-permute-start(bf16[112,192]{1,0:T(8,128)(2,1)} %get-tuple-element.24), channel_id=1, source_target_pairs={{0,16},{8,24},{16,32},{24,40},{32,48},{40,56},{48,64},{56,72},{64,... | collective-permute-start | bytes 129032 | tf_op jit(solution)/shard_map/ppermute | solution.py:472
  25.0 14.6 %collective-permute-start.2 = (bf16[112,192]{1,0:T(8,128)(2,1)}, bf16[112,192]{1,0:T(8,128)(2,1)S(1)}, u32[]{:S(2)}, u32[]{:S(2)}) collective-permute-start(bf16[112,192]{1,0:T(8,128)(2,1)} %get-tuple-element.24), channel_id=1, source_target_pairs={{0,24},{8,32},{16,40},{24,48},{32,56},{40,64},{48,72},{56,80},{64,... | collective-permute-start | bytes 129032 | tf_op jit(solution)/shard_map/ppermute | solution.py:472
  29.7 10.0 %collective-permute-start.3 = (bf16[112,192]{1,0:T(8,128)(2,1)}, bf16[112,192]{1,0:T(8,128)(2,1)S(1)}, u32[]{:S(2)}, u32[]{:S(2)}) collective-permute-start(bf16[112,192]{1,0:T(8,128)(2,1)} %get-tuple-element.24), channel_id=1, source_target_pairs={{0,32},{8,40},{16,48},{24,56},{32,64},{40,72},{48,80},{56,88},{64,... | collective-permute-start | bytes 129032 | tf_op jit(solution)/shard_map/ppermute | solution.py:472
  48.3 2.0 copy-start.4
  49.9 4.6 %copy-start.3 = (bf16[4,768,384]{2,1,0:T(8,128)(2,1)S(1)}, bf16[4,768,384]{2,1,0:T(8,128)(2,1)}, u32[]{:S(2)}) copy-start(bf16[4,768,384]{2,1,0:T(8,128)(2,1)} %get-tuple-element.25) | copy-start | bytes 7077892
  49.9 8.0 %collective-permute-start.5 = (bf16[2,768,384]{2,1,0:T(8,128)(2,1)S(1)}, bf16[2,768,384]{2,1,0:T(8,128)(2,1)S(1)}, u32[]{:S(2)}, u32[]{:S(2)}) collective-permute-start(bf16[2,768,384]{2,1,0:T(8,128)(2,1)S(1)} %slice.99), channel_id=1, source_target_pairs={{0,1},{1,0},{2,3},{3,2},{4,5},{5,4},{6,7},{7,6},{8,9},{9,8},{10,11... | collective-permute-start | bytes 3538952 | tf_op jit(solution)/shard_map/ppermute | solution.py:381
  50.4 3.2 %collective-permute-start.4 = (bf16[768,384]{1,0:T(8,128)(2,1)S(1)}, bf16[768,384]{1,0:T(8,128)(2,1)S(1)}, u32[]{:S(2)}, u32[]{:S(2)}) collective-permute-start(bf16[768,384]{1,0:T(8,128)(2,1)S(1)} %get-tuple-element.44), channel_id=1, source_target_pairs={{0,1},{1,0},{2,3},{3,2},{4,5},{5,4},{6,7},{7,6},{8,9},{9,8},{10,11... | collective-permute-start | bytes 1769480 | tf_op jit(solution)/shard_map/ppermute | solution.py:381
  50.7 3.8 %collective-permute-start.6 = (bf16[768,384]{1,0:T(8,128)(2,1)S(1)}, bf16[768,384]{1,0:T(8,128)(2,1)S(1)}, u32[]{:S(2)}, u32[]{:S(2)}) collective-permute-start(bf16[768,384]{1,0:T(8,128)(2,1)S(1)} %get-tuple-element.43), channel_id=1, source_target_pairs={{0,1},{1,0},{2,3},{3,2},{4,5},{5,4},{6,7},{7,6},{8,9},{9,8},{10,11... | collective-permute-start | bytes 1769480 | tf_op jit(solution)/shard_map/ppermute | solution.py:381
  54.8 9.6 %collective-permute-start.11 = (bf16[384,384]{1,0:T(8,128)(2,1)S(1)}, bf16[384,384]{1,0:T(8,128)(2,1)S(1)}, u32[]{:S(2)}, u32[]{:S(2)}) collective-permute-start(bf16[384,384]{1,0:T(8,128)(2,1)S(1)} %get-tuple-element.52), channel_id=1, source_target_pairs={{0,6},{2,0},{4,2},{6,4},{1,7},{3,1},{5,3},{7,5},{8,14},{10,8},{12,... | collective-permute-start | bytes 884744 | tf_op jit(solution)/shard_map/ppermute | solution.py:377
  57.9 10.5 %collective-permute-start.7 = (bf16[384,384]{1,0:T(8,128)(2,1)S(1)}, bf16[384,384]{1,0:T(8,128)(2,1)S(1)}, u32[]{:S(2)}, u32[]{:S(2)}) collective-permute-start(bf16[384,384]{1,0:T(8,128)(2,1)S(1)} %get-tuple-element.51), channel_id=1, source_target_pairs={{0,2},{2,4},{4,6},{6,0},{1,3},{3,5},{5,7},{7,1},{8,10},{10,12},{12... | collective-permute-start | bytes 884744 | tf_op jit(solution)/shard_map/ppermute | solution.py:377
  64.5 11.2 %collective-permute-start.12 = (bf16[384,384]{1,0:T(8,128)(2,1)S(1)}, bf16[384,384]{1,0:T(8,128)(2,1)S(1)}, u32[]{:S(2)}, u32[]{:S(2)}) collective-permute-start(bf16[384,384]{1,0:T(8,128)(2,1)S(1)} %fusion.8), channel_id=1, source_target_pairs={{0,6},{2,0},{4,2},{6,4},{1,7},{3,1},{5,3},{7,5},{8,14},{10,8},{12,... | collective-permute-start | bytes 884744 | tf_op jit(solution)/shard_map/ppermute | solution.py:377
  68.4 11.2 %collective-permute-start.8 = (bf16[384,384]{1,0:T(8,128)(2,1)S(1)}, bf16[384,384]{1,0:T(8,128)(2,1)S(1)}, u32[]{:S(2)}, u32[]{:S(2)}) collective-permute-start(bf16[384,384]{1,0:T(8,128)(2,1)S(1)} %fusion.9), channel_id=1, source_target_pairs={{0,2},{2,4},{4,6},{6,0},{1,3},{3,5},{5,7},{7,1},{8,10},{10,12},{12... | collective-permute-start | bytes 884744 | tf_op jit(solution)/shard_map/ppermute | solution.py:377
  68.5 15.5 %collective-permute-start.10 = (bf16[384,384]{1,0:T(8,128)(2,1)S(1)}, bf16[384,384]{1,0:T(8,128)(2,1)S(1)}, u32[]{:S(2)}, u32[]{:S(2)}) collective-permute-start(bf16[384,384]{1,0:T(8,128)(2,1)S(1)} %slice_bitcast_fusion.3), channel_id=1, source_target_pairs={{0,2},{2,4},{4,6},{6,0},{1,3},{3,5},{5,7},{7,1},{8,10},{10,12},{12... | collective-permute-start | bytes 884744 | tf_op jit(solution)/shard_map/ppermute | solution.py:377
  68.6 15.5 %collective-permute-start.9 = (bf16[384,384]{1,0:T(8,128)(2,1)S(1)}, bf16[384,384]{1,0:T(8,128)(2,1)S(1)}, u32[]{:S(2)}, u32[]{:S(2)}) collective-permute-start(bf16[384,384]{1,0:T(8,128)(2,1)S(1)} %slice_bitcast_fusion.4), channel_id=1, source_target_pairs={{0,6},{2,0},{4,2},{6,4},{1,7},{3,1},{5,3},{7,5},{8,14},{10,8},{12,... | collective-permute-start | bytes 884744 | tf_op jit(solution)/shard_map/ppermute | solution.py:377
  85.3 23.2 %slice-start.1 = ((f32[3,1056]{1,0:T(4,128)}), f32[3,32]{1,0:T(4,128)S(1)}, s32[]{:S(2)}) async-start(f32[3,1056]{1,0:T(4,128)} %param.34), calls=%async_computation.2 | async-start | bytes 4096 | tf_op jit(solution)/shard_map/slice | solution.py:454
  85.3 23.2 %copy-start.17 = (s32[8]{0:T(128)S(1)}, s32[8]{0:T(128)}, u32[]{:S(2)}) copy-start(s32[8]{0:T(128)} %constant.52.clone) | copy-start | bytes 100
  85.3 23.2 %copy-start.18 = (s32[8]{0:T(128)S(1)}, s32[8]{0:T(128)}, u32[]{:S(2)}) copy-start(s32[8]{0:T(128)} %constant.53.clone) | copy-start | bytes 100
  85.3 23.2 %copy-start.15 = (s32[8]{0:T(128)S(1)}, s32[8]{0:T(128)}, u32[]{:S(2)}) copy-start(s32[8]{0:T(128)} %constant.54.clone) | copy-start | bytes 100
  85.3 23.2 %copy-start.16 = (s32[8]{0:T(128)S(1)}, s32[8]{0:T(128)}, u32[]{:S(2)}) copy-start(s32[8]{0:T(128)} %constant.55.clone) | copy-start | bytes 100
  85.3 25.1 %copy-start.1 = (f32[3072]{0:T(1024)S(1)}, f32[3072]{0:T(1024)}, u32[]{:S(2)}) copy-start(f32[3072]{0:T(1024)} %param.31) | copy-start | bytes 36868
  85.3 14.9 %collective-permute-start.13 = (bf16[768,384]{1,0:T(8,128)(2,1)S(1)}, bf16[768,384]{1,0:T(8,128)(2,1)S(1)}, u32[]{:S(2)}, u32[]{:S(2)}) collective-permute-start(bf16[768,384]{1,0:T(8,128)(2,1)S(1)} %fusion.3.refs_0_), channel_id=1, source_target_pairs={{0,2},{2,4},{4,6},{6,0},{1,3},{3,5},{5,7},{7,1},{8,10},{10,12},{12... | collective-permute-start | bytes 1769480 | tf_op jit(solution)/shard_map/ppermute | solution.py:377
  85.4 14.9 %collective-permute-start.14 = (bf16[768,384]{1,0:T(8,128)(2,1)S(1)}, bf16[768,384]{1,0:T(8,128)(2,1)S(1)}, u32[]{:S(2)}, u32[]{:S(2)}) collective-permute-start(bf16[768,384]{1,0:T(8,128)(2,1)S(1)} %fusion.3.refs_0_), channel_id=1, source_target_pairs={{0,6},{2,0},{4,2},{6,4},{1,7},{3,1},{5,3},{7,5},{8,14},{10,8},{12,... | collective-permute-start | bytes 1769480 | tf_op jit(solution)/shard_map/ppermute | solution.py:377
  100.2 8.0 %collective-permute-start.15 = (bf16[384,384]{1,0:T(8,128)(2,1)S(1)}, bf16[384,384]{1,0:T(8,128)(2,1)S(1)}, u32[]{:S(2)}, u32[]{:S(2)}) collective-permute-start(bf16[384,384]{1,0:T(8,128)(2,1)S(1)} %slice.136), channel_id=1, source_target_pairs={{0,2},{2,4},{4,6},{6,0},{1,3},{3,5},{5,7},{7,1},{8,10},{10,12},{12... | collective-permute-start | bytes 884744 | tf_op jit(solution)/shard_map/ppermute | solution.py:377
  100.4 7.9 %collective-permute-start.16 = (bf16[384,384]{1,0:T(8,128)(2,1)S(1)}, bf16[384,384]{1,0:T(8,128)(2,1)S(1)}, u32[]{:S(2)}, u32[]{:S(2)}) collective-permute-start(bf16[384,384]{1,0:T(8,128)(2,1)S(1)} %slice.137), channel_id=1, source_target_pairs={{0,6},{2,0},{4,2},{6,4},{1,7},{3,1},{5,3},{7,5},{8,14},{10,8},{12,... | collective-permute-start | bytes 884744 | tf_op jit(solution)/shard_map/ppermute | solution.py:377
  103.6 5.5 %collective-permute-start.17 = (bf16[768,384]{1,0:T(8,128)(2,1)S(1)}, bf16[768,384]{1,0:T(8,128)(2,1)S(1)}, u32[]{:S(2)}, u32[]{:S(2)}) collective-permute-start(bf16[768,384]{1,0:T(8,128)(2,1)S(1)} %fusion.3.refs_0_), channel_id=1, source_target_pairs={{0,1},{1,0},{2,3},{3,2},{4,5},{5,4},{6,7},{7,6},{8,9},{9,8},{10,11... | collective-permute-start | bytes 1769480 | tf_op jit(solution)/shard_map/ppermute | solution.py:381
  103.7 5.5 %collective-permute-start.18 = (bf16[768,384]{1,0:T(8,128)(2,1)S(1)}, bf16[768,384]{1,0:T(8,128)(2,1)S(1)}, u32[]{:S(2)}, u32[]{:S(2)}) collective-permute-start(bf16[768,384]{1,0:T(8,128)(2,1)S(1)} %collective-permute-done.13.refs_1_), channel_id=1, source_target_pairs={{0,1},{1,0},{2,3},{3,2},{4,5},{5,4},{6,7},{7,6},{8,9},{9,8},{10,11... | collective-permute-start | bytes 1769480 | tf_op jit(solution)/shard_map/ppermute | solution.py:381
  104.2 5.0 %collective-permute-start.19 = (bf16[768,384]{1,0:T(8,128)(2,1)S(1)}, bf16[768,384]{1,0:T(8,128)(2,1)S(1)}, u32[]{:S(2)}, u32[]{:S(2)}) collective-permute-start(bf16[768,384]{1,0:T(8,128)(2,1)S(1)} %collective-permute-done.14.refs_2_), channel_id=1, source_target_pairs={{0,1},{1,0},{2,3},{3,2},{4,5},{5,4},{6,7},{7,6},{8,9},{9,8},{10,11... | collective-permute-start | bytes 1769480 | tf_op jit(solution)/shard_map/ppermute | solution.py:381
  108.3 2.1 collective-permute-start.20
  110.4 7.9 %slice-start = ((f32[3,1056]{1,0:T(4,128)}), f32[3,1024]{1,0:T(4,128)S(1)}, s32[]{:S(2)}) async-start(f32[3,1056]{1,0:T(4,128)} %param.34), calls=%async_computation.1 | async-start | bytes 32768 | tf_op jit(solution)/shard_map/slice | solution.py:453
  115.8 7.6 %collective-permute-start.21 = (bf16[16,3072]{1,0:T(8,128)(2,1)S(1)}, bf16[16,3072]{1,0:T(8,128)(2,1)S(1)}, u32[]{:S(2)}, u32[]{:S(2)}) collective-permute-start(bf16[16,3072]{1,0:T(8,128)(2,1)S(1)} %get-tuple-element.28), channel_id=1, source_target_pairs={{0,8},{8,16},{16,24},{24,32},{32,40},{40,48},{48,56},{56,64},{64,7... | collective-permute-start | bytes 294920 | tf_op jit(solution)/shard_map/ppermute | solution.py:544
  166.2 2.3 %collective-permute-start.24 = (bf16[768,384]{1,0:T(8,128)(2,1)}, bf16[768,384]{1,0:T(8,128)(2,1)S(1)}, u32[]{:S(2)}, u32[]{:S(2)}) collective-permute-start(bf16[768,384]{1,0:T(8,128)(2,1)} %bitcast.40), channel_id=1, source_target_pairs={{0,1},{1,0},{2,3},{3,2},{4,5},{5,4},{6,7},{7,6},{8,9},{9,8},{10,11... | collective-permute-start | bytes 1769480 | tf_op jit(solution)/shard_map/ppermute | solution.py:381
  166.3 10.5 %collective-permute-start.23 = (bf16[2,768,384]{2,1,0:T(8,128)(2,1)}, bf16[2,768,384]{2,1,0:T(8,128)(2,1)S(1)}, u32[]{:S(2)}, u32[]{:S(2)}) collective-permute-start(bf16[2,768,384]{2,1,0:T(8,128)(2,1)} %get-tuple-element.34), channel_id=1, source_target_pairs={{0,1},{1,0},{2,3},{3,2},{4,5},{5,4},{6,7},{7,6},{8,9},{9,8},{10,11... | collective-permute-start | bytes 3538952 | tf_op jit(solution)/shard_map/ppermute | solution.py:381
  168.5 4.5 %copy-start = (bf16[768,1152]{1,0:T(8,128)(2,1)S(1)}, bf16[768,1152]{1,0:T(8,128)(2,1)}, u32[]{:S(2)}) copy-start(bf16[768,1152]{1,0:T(8,128)(2,1)} %get-tuple-element.31.h_ref) | copy-start | bytes 5308420
  168.5 4.5 %copy-start.2 = (s32[8]{0:T(128)S(1)}, s32[8]{0:T(128)}, u32[]{:S(2)}) copy-start(s32[8]{0:T(128)} %fusion.15.order_ref) | copy-start | bytes 100
  169.9 10.6 %collective-permute-start.29 = (bf16[384,384]{1,0:T(8,128)(2,1)S(1)}, bf16[384,384]{1,0:T(8,128)(2,1)S(1)}, u32[]{:S(2)}, u32[]{:S(2)}) collective-permute-start(bf16[384,384]{1,0:T(8,128)(2,1)S(1)} %get-tuple-element.50), channel_id=1, source_target_pairs={{0,6},{2,0},{4,2},{6,4},{1,7},{3,1},{5,3},{7,5},{8,14},{10,8},{12,... | collective-permute-start | bytes 884744 | tf_op jit(solution)/shard_map/ppermute | solution.py:377
  176.6 14.1 %collective-permute-start.22 = (bf16[768,384]{1,0:T(8,128)(2,1)S(1)}, bf16[768,384]{1,0:T(8,128)(2,1)S(1)}, u32[]{:S(2)}, u32[]{:S(2)}) collective-permute-start(bf16[768,384]{1,0:T(8,128)(2,1)S(1)} %get-tuple-element.33), channel_id=1, source_target_pairs={{0,1},{1,0},{2,3},{3,2},{4,5},{5,4},{6,7},{7,6},{8,9},{9,8},{10,11... | collective-permute-start | bytes 1769480 | tf_op jit(solution)/shard_map/ppermute | solution.py:381
  176.7 10.6 %collective-permute-start.25 = (bf16[384,384]{1,0:T(8,128)(2,1)S(1)}, bf16[384,384]{1,0:T(8,128)(2,1)S(1)}, u32[]{:S(2)}, u32[]{:S(2)}) collective-permute-start(bf16[384,384]{1,0:T(8,128)(2,1)S(1)} %get-tuple-element.49), channel_id=1, source_target_pairs={{0,2},{2,4},{4,6},{6,0},{1,3},{3,5},{5,7},{7,1},{8,10},{10,12},{12... | collective-permute-start | bytes 884744 | tf_op jit(solution)/shard_map/ppermute | solution.py:377
  180.6 10.2 %collective-permute-start.30 = (bf16[384,384]{1,0:T(8,128)(2,1)S(1)}, bf16[384,384]{1,0:T(8,128)(2,1)S(1)}, u32[]{:S(2)}, u32[]{:S(2)}) collective-permute-start(bf16[384,384]{1,0:T(8,128)(2,1)S(1)} %add_convert_fusion.2), channel_id=1, source_target_pairs={{0,6},{2,0},{4,2},{6,4},{1,7},{3,1},{5,3},{7,5},{8,14},{10,8},{12,... | collective-permute-start | bytes 884744 | tf_op jit(solution)/shard_map/ppermute | solution.py:377
  187.4 11.2 %collective-permute-start.26 = (bf16[384,384]{1,0:T(8,128)(2,1)S(1)}, bf16[384,384]{1,0:T(8,128)(2,1)S(1)}, u32[]{:S(2)}, u32[]{:S(2)}) collective-permute-start(bf16[384,384]{1,0:T(8,128)(2,1)S(1)} %add_convert_fusion.3), channel_id=1, source_target_pairs={{0,2},{2,4},{4,6},{6,0},{1,3},{3,5},{5,7},{7,1},{8,10},{10,12},{12... | collective-permute-start | bytes 884744 | tf_op jit(solution)/shard_map/ppermute | solution.py:377
  187.5 11.1 %collective-permute-start.27 = (bf16[384,384]{1,0:T(8,128)(2,1)S(1)}, bf16[384,384]{1,0:T(8,128)(2,1)S(1)}, u32[]{:S(2)}, u32[]{:S(2)}) collective-permute-start(bf16[384,384]{1,0:T(8,128)(2,1)S(1)} %slice.121), channel_id=1, source_target_pairs={{0,6},{2,0},{4,2},{6,4},{1,7},{3,1},{5,3},{7,5},{8,14},{10,8},{12,... | collective-permute-start | bytes 884744 | tf_op jit(solution)/shard_map/ppermute | solution.py:377
  190.7 12.8 %collective-permute-start.28 = (bf16[384,384]{1,0:T(8,128)(2,1)S(1)}, bf16[384,384]{1,0:T(8,128)(2,1)S(1)}, u32[]{:S(2)}, u32[]{:S(2)}) collective-permute-start(bf16[384,384]{1,0:T(8,128)(2,1)S(1)} %slice.123), channel_id=1, source_target_pairs={{0,2},{2,4},{4,6},{6,0},{1,3},{3,5},{5,7},{7,1},{8,10},{10,12},{12... | collective-permute-start | bytes 884744 | tf_op jit(solution)/shard_map/ppermute | solution.py:377
  (7 other events, 6.5 us)
Sparse Core Ops, SparseCore 0:
  10.0 132.0 all-gather.1
